TPU v7x, 32 devices: a whole 2x2x4 slice. The times are simulated.
32 devices in a mesh: sp: 8 (over z, x), tp: 4 (over y, core).
Axes of the slice: x: 2, y: 2, z: 4, core: 2. Of those that a mesh axis runs over, the one named last changes fastest.
Arguments:
- cotangent: bfloat16 [1536, 2048], P('sp'), may hold values from -8 to 8
- residual: bfloat16 [1536, 2048], P('sp'), may hold values from -6 to 6
- norm_gain: float32 [2048], replicated, may hold values from 0.1 to 1.9
- route_ids: int32 [1536, 2], P('sp'), may hold values from 0 to 7, all different within a row; in each aligned block of 192 rows (0 to 191, 192 to 383, ...) at most 96 rows name the same one
- route_weights: float32 [1536, 2], P('sp'), may hold values from 0.1 to 1
- expert_gate: bfloat16 [8, 2048, 1024], P('sp', None, 'tp'), may hold values from -0.125 to 0.125
- expert_up: bfloat16 [8, 2048, 1024], P('sp', None, 'tp'), may hold values from -0.125 to 0.125
- expert_down: bfloat16 [8, 1024, 2048], P('sp', 'tp'), may hold values from -0.1875 to 0.1875
- out_proj: bfloat16 [2048, 1024], P(None, 'tp'), may hold values from -0.1875 to 0.1875
- conv_out: bfloat16 [1536, 1024], P('sp', 'tp'), may hold values from -6 to 6, as said below
- branch_gate: bfloat16 [1536, 1024], P('sp', 'tp'), may hold values from -6 to 6
- prev_state: bfloat16 [1536, 1024], P('sp', 'tp'), may hold values from -6 to 6
- decay_param: float32 [1024], P('tp'), as said below
- rate_map: bfloat16 [16, 64, 64], P('tp'), may hold values from -0.75 to 0.75
- input_map: bfloat16 [16, 64, 64], P('tp'), may hold values from -0.75 to 0.75
Outputs:
- grad_gate: float32 [8, 2048, 1024], P('sp', None, 'tp')
- grad_up: float32 [8, 2048, 1024], P('sp', None, 'tp')
- grad_down: float32 [8, 1024, 2048], P('sp', 'tp')
- grad_out_proj: float32 [2048, 1024], P('sp', 'tp')
- grad_conv_out: float32 [1536, 1024], P('sp', 'tp')
- grad_branch_gate: float32 [1536, 1024], P('sp', 'tp')
Inputs may be any that keep to these rules, and one draw needn't show every extreme that they name: `route_ids`: within the rows of one device (aligned blocks of 192 rows) no expert is named by more than 96 rows, a bound that some block reaches; the two ids of a row differ. `conv_out`: every entry is a finite value between -6 and 6. `decay_param`: every channel's decay parameter is at least 4.
All inputs are finite; a program needn't handle non-finite values.
Results may differ from a plain program's by a relative error of at most 0.0095.
Values may be sent and summed in bfloat16 or wider, within the bound.
A program may use at most 128 MiB of HBM per device.

v0:
```python
import jax
import jax.numpy as jnp
from jax import lax
from jax.sharding import PartitionSpec as P

RATE_SCALE = 8.0
NORM_EPS = 1e-06
SERIES_EDGE = 0.001


def entering(part, axis, combine, identity):
    count = lax.axis_size(axis)
    place = lax.axis_index(axis)
    ahead = count - 1 - place
    gathered = jax.tree.map(lambda a: lax.all_gather(a, axis), part)
    state = jax.tree.map(lambda a, e: jnp.zeros_like(a) + jnp.asarray(e, a.dtype), part, identity)

    def one(turn, state):
        source = count - 1 - turn
        return combine(
            state, jax.tree.map(lambda a: lax.dynamic_index_in_dim(a, source, 0, False), gathered)
        )

    return lax.fori_loop(0, ahead, one, state)


def gelu_pair(values):
    result, pullback = jax.vjp(jax.nn.gelu, values)
    return (result, pullback(jnp.ones_like(values))[0])


def gate_maps(conv_out, weights):
    rows_here = conv_out.shape[0]
    blocked = conv_out.reshape(rows_here, weights.shape[0], weights.shape[1])
    mapped = jnp.einsum("tbi,bij->tbj", blocked, weights, preferred_element_type=jnp.float32)
    return mapped.reshape(rows_here, -1)


def gate_maps_back(grad_values, weights):
    rows_here = grad_values.shape[0]
    blocked = grad_values.reshape(rows_here, weights.shape[0], weights.shape[2])
    mapped = jnp.einsum(
        "tbj,bij->tbi", blocked, weights.astype(jnp.float32), precision=lax.Precision.HIGHEST
    )
    return mapped.reshape(rows_here, -1)


def norm_slope(spread):
    tiny_side = spread < SERIES_EDGE
    denominator = jnp.where(tiny_side, 1.0, -jnp.expm1(-spread))
    series_ratio = jnp.where(tiny_side, 1.0 + 0.5 * spread, spread / denominator)
    return 0.5 * jnp.sqrt(spread * series_ratio)


def reverse_linear(factors, term_values):

    def combine(left_pair, right_pair):
        return (left_pair[0] * right_pair[0], right_pair[0] * left_pair[1] + right_pair[1])

    flipped = lax.associative_scan(
        combine, (jnp.flip(factors, 0), jnp.flip(term_values, 0)), axis=0
    )
    return jnp.flip(flipped[1], 0)


def per_device(
    cotangent,
    residual,
    norm_gain,
    route_ids,
    route_weights,
    expert_gate,
    expert_up,
    expert_down,
    out_proj,
    conv_out,
    branch_gate,
    prev_state,
    decay_param,
    rate_map,
    input_map,
):
    tok_rows, model_width = residual.shape
    sp_count = lax.axis_size("sp")
    tp_count = lax.axis_size("tp")
    local_experts = expert_gate.shape[0]
    experts_all = local_experts * sp_count
    capacity = 4 * tok_rows // experts_all
    slot_total = experts_all * capacity
    res_values = residual.astype(jnp.float32)
    inv_rms = lax.rsqrt(jnp.mean(res_values * res_values, axis=1, keepdims=True) + NORM_EPS)
    moe_input = (res_values * inv_rms * norm_gain[None, :]).astype(jnp.bfloat16)
    scaled_cot = (route_weights[:, :, None] * cotangent.astype(jnp.float32)[:, None, :]).astype(
        jnp.bfloat16
    )
    scaled_cot = scaled_cot.reshape(2 * tok_rows, model_width)
    flat_ids = route_ids.reshape(-1)
    expert_hits = (flat_ids[:, None] == jnp.arange(experts_all, dtype=jnp.int32)[None, :]).astype(
        jnp.int32
    )
    earlier_hits = jnp.cumsum(expert_hits, axis=0) - expert_hits
    slot_pos = flat_ids * capacity + jnp.sum(earlier_hits * expert_hits, axis=1)
    slot_match = slot_pos[None, :] == jnp.arange(slot_total, dtype=jnp.int32)[:, None]
    source_row = jnp.sum(
        jnp.where(slot_match, jnp.arange(2 * tok_rows, dtype=jnp.int32)[None, :], 0), axis=1
    )
    filled = jnp.any(slot_match, axis=1)
    cot_send = jnp.where(filled[:, None], scaled_cot[source_row], jnp.zeros((), jnp.bfloat16))
    cot_send = cot_send.reshape(experts_all, capacity, model_width)
    rows_send = moe_input[source_row // 2].reshape(experts_all, capacity, model_width)
    part_cols = model_width // tp_count
    col_start = lax.axis_index("tp") * part_cols
    cot_part = lax.dynamic_slice_in_dim(cot_send, col_start, part_cols, 2)
    rows_part = lax.dynamic_slice_in_dim(rows_send, col_start, part_cols, 2)
    cot_part, rows_part = (
        lax.all_to_all(cot_part, "sp", split_axis=0, concat_axis=0, tiled=True),
        lax.all_to_all(rows_part, "sp", split_axis=0, concat_axis=0, tiled=True),
    )
    cot_recv, rows_recv = (
        lax.all_gather(cot_part, "tp", axis=2, tiled=True),
        lax.all_gather(rows_part, "tp", axis=2, tiled=True),
    )

    def to_expert_rows(slots):
        shaped = slots.reshape(sp_count, local_experts, capacity, slots.shape[2])
        return jnp.transpose(shaped, (1, 0, 2, 3)).reshape(
            local_experts, sp_count * capacity, slots.shape[2]
        )

    rows_in = to_expert_rows(rows_recv)
    cot_in = to_expert_rows(cot_recv)
    gate_pre = jnp.einsum("erd,edf->erf", rows_in, expert_gate, preferred_element_type=jnp.float32)
    up_pre = jnp.einsum("erd,edf->erf", rows_in, expert_up, preferred_element_type=jnp.float32)
    gate_sig = jax.nn.sigmoid(gate_pre)
    gate_act = gate_pre * gate_sig
    hidden = (gate_act * up_pre).astype(jnp.bfloat16)
    d_hidden = jnp.einsum("erd,efd->erf", cot_in, expert_down, preferred_element_type=jnp.float32)
    d_up = (d_hidden * gate_act).astype(jnp.bfloat16)
    d_gate = (d_hidden * up_pre * gate_sig * (1.0 + gate_pre * (1.0 - gate_sig))).astype(
        jnp.bfloat16
    )
    grad_down = jnp.einsum("erf,erd->efd", hidden, cot_in, preferred_element_type=jnp.float32)
    grad_gate = jnp.einsum("erd,erf->edf", rows_in, d_gate, preferred_element_type=jnp.float32)
    grad_up = jnp.einsum("erd,erf->edf", rows_in, d_up, preferred_element_type=jnp.float32)
    back_terms = jnp.einsum("erf,edf->erd", d_gate, expert_gate, preferred_element_type=jnp.float32)
    back_terms = back_terms + jnp.einsum(
        "erf,edf->erd", d_up, expert_up, preferred_element_type=jnp.float32
    )
    back_terms = back_terms.astype(jnp.bfloat16)
    back_terms = jnp.transpose(
        back_terms.reshape(local_experts, sp_count, capacity, model_width), (1, 0, 2, 3)
    )
    back_terms = back_terms.reshape(sp_count * local_experts, capacity, model_width)
    summed = (
        lax.psum_scatter(back_terms, "tp", scatter_dimension=2, tiled=True)
        .astype(jnp.float32)
        .astype(jnp.bfloat16)
    )
    returned = lax.all_to_all(summed, "sp", split_axis=0, concat_axis=0, tiled=True)
    returned = lax.all_gather(returned, "tp", axis=2, tiled=True)
    back_rows = returned.reshape(slot_total, model_width)[slot_pos].astype(jnp.float32)
    d_normed = jnp.sum(back_rows.reshape(tok_rows, 2, model_width), axis=1)
    weighted = norm_gain[None, :] * d_normed
    cubed = inv_rms * inv_rms * inv_rms
    d_mix = (
        cotangent.astype(jnp.float32)
        + inv_rms * weighted
        - res_values * cubed * jnp.mean(res_values * weighted, axis=1, keepdims=True)
    ).astype(jnp.bfloat16)
    rate_gate = jax.nn.sigmoid(gate_maps(conv_out, rate_map))
    input_gate = jax.nn.sigmoid(gate_maps(conv_out, input_map))
    soft_decay = jax.nn.softplus(-decay_param)
    log_keep = -RATE_SCALE * rate_gate * soft_decay[None, :]
    keep_rate = jnp.exp(log_keep)
    spread = -2.0 * log_keep
    norm_term = jnp.sqrt(-jnp.expm1(-spread))
    conv_values = conv_out.astype(jnp.float32)
    prev_values = prev_state.astype(jnp.float32)
    state_now = keep_rate * prev_values + norm_term * input_gate * conv_values
    gelu_value, gelu_slope = gelu_pair(branch_gate.astype(jnp.float32))
    branch_out = (state_now * gelu_value).astype(jnp.bfloat16)
    grad_out_proj = lax.psum_scatter(
        lax.dot_general(
            d_mix, branch_out, (((0,), (0,)), ((), ())), preferred_element_type=jnp.float32
        ),
        "sp",
        scatter_dimension=0,
        tiled=True,
    )
    d_branch = jnp.dot(d_mix, out_proj, preferred_element_type=jnp.float32)
    next_keep = jnp.concatenate([keep_rate[1:], jnp.zeros_like(keep_rate[:1])], axis=0)
    local_grad = reverse_linear(next_keep, d_branch * gelu_value)
    next_log = jnp.concatenate([log_keep[1:], jnp.zeros_like(log_keep[:1])], axis=0)
    tail_keep = jnp.exp(jnp.flip(jnp.cumsum(jnp.flip(next_log, 0), axis=0), 0))
    block_keep = jnp.exp(jnp.sum(log_keep, axis=0))
    head_term = keep_rate[0] * local_grad[0]

    def compose(earlier, later_part):
        return (later_part[0] * earlier[0], later_part[0] * earlier[1] + later_part[1])

    carried = entering(
        (block_keep, head_term),
        "sp",
        compose,
        (jnp.ones_like(block_keep), jnp.zeros_like(head_term)),
    )
    state_grad = local_grad + tail_keep * carried[1][None, :]
    grad_branch_gate = d_branch * state_now * gelu_slope
    keep_grad = state_grad * prev_values * keep_rate
    inner_input = input_gate * conv_values
    rate_back = keep_grad * (-RATE_SCALE * soft_decay[None, :]) * rate_gate * (1.0 - rate_gate)
    rate_back = rate_back + state_grad * inner_input * keep_rate * keep_rate * (
        1.0 - rate_gate
    ) * norm_slope(spread)
    input_back = state_grad * norm_term * conv_values * input_gate * (1.0 - input_gate)
    grad_conv_out = (
        state_grad * norm_term * input_gate
        + gate_maps_back(rate_back, rate_map)
        + gate_maps_back(input_back, input_map)
    )
    return (grad_gate, grad_up, grad_down, grad_out_proj, grad_conv_out, grad_branch_gate)


def solution(mesh):
    in_specs = (
        P("sp", None),
        P("sp", None),
        P(),
        P("sp", None),
        P("sp", None),
        P("sp", None, "tp"),
        P("sp", None, "tp"),
        P("sp", "tp", None),
        P(None, "tp"),
        P("sp", "tp"),
        P("sp", "tp"),
        P("sp", "tp"),
        P("tp"),
        P("tp", None, None),
        P("tp", None, None),
    )
    out_specs = (
        P("sp", None, "tp"),
        P("sp", None, "tp"),
        P("sp", "tp", None),
        P("sp", "tp"),
        P("sp", "tp"),
        P("sp", "tp"),
    )
    return jax.shard_map(
        per_device, mesh=mesh, in_specs=in_specs, out_specs=out_specs, check_vma=False
    )
```

profile of v0, /device:TPU:0, one launch (start us, length us, event | category | flops | bytes accessed | tf_op | source)
XLA Modules:
  0.0 328.5 jit_solution(5379476029609607391)
XLA Ops:
  7.2 0.9 copy.81
  8.1 0.1 eq.39
  8.3 0.1 reshape.304
  8.4 1.4 fusion
  9.8 0.9 reduce-window.14
  10.7 0.2 slice_reduce_fusion
  11.0 0.2 select_reduce_fusion
  11.3 1.4 fusion.2
  12.7 4.2 %gather_fusion = bf16[768,2048]{1,0:T(8,128)(2,1)} fusion(bf16[192,2048]{1,0:T(8,128)(2,1)S(1)} %fusion.2, s32[1024]{0:T(1024)S(1)} %get-tuple-element.138), kind=kCustom, calls=%fused_computation | custom fusion | bytes 6294528 | tf_op jit(solution)/shard_map/gather | solution.py:110
  16.9 1.3 constant_dynamic-slice_fusion.2
  18.2 27.3 %all_to_all.15 = bf16[8,96,512]{2,1,0:T(8,128)(2,1)} all-to-all(bf16[8,96,512]{2,1,0:T(8,128)(2,1)S(1)} %constant_dynamic-slice_fusion.2), channel_id=1, replica_groups=mesh['sp'=8,'tp'=4] {'sp'}, dimensions={0} | all-to-all | bytes 1572864 | tf_op jit(solution)/shard_map/all_to_all | solution.py:117
  45.6 3.3 mul.385
  48.9 5.5 %mul.386 = f32[384,2048]{1,0:T(8,128)} reshape(f32[192,2,2048]{2,1,0:T(2,128)} %mul.385) | data formatting | bytes 6291456 | tf_op jit(solution)/shard_map/mul | solution.py:93
  54.5 0.1 mul.383
  54.7 0.2 fusion.7
  55.0 2.1 multiply_convert_fusion
  57.1 4.3 %gather_fusion.1 = bf16[768,2048]{1,0:T(8,128)(2,1)} fusion(bf16[384,2048]{1,0:T(8,128)(2,1)S(1)} %multiply_convert_fusion, s32[1024]{0:T(1024)S(1)} %get-tuple-element.137), kind=kCustom, calls=%fused_computation.1 | custom fusion | bytes 6294528 | tf_op jit(solution)/shard_map/gather | solution.py:108
  61.4 1.4 dynamic-slice_select_fusion
  62.8 23.6 %all_to_all.16 = bf16[8,96,512]{2,1,0:T(8,128)(2,1)} all-to-all(bf16[8,96,512]{2,1,0:T(8,128)(2,1)S(1)} %dynamic-slice_select_fusion), channel_id=1, replica_groups=mesh['sp'=8,'tp'=4] {'sp'}, dimensions={0} | all-to-all | bytes 1572864 | tf_op jit(solution)/shard_map/all_to_all | solution.py:116
  86.5 3.0 fusion.16
  89.7 1.9 fusion.19
  91.6 22.6 %all-gather.8.cloned.1.call-done = bf16[8,96,2048]{2,1,0:T(8,128)(2,1)} async-done(((bf16[8,96,512]{2,1,0:T(8,128)(2,1)}), bf16[8,96,2048]{2,1,0:T(8,128)(2,1)}) %all-gather.8.cloned.1.call-update) | async-done | bytes 3145744 | tf_op jit(solution)/shard_map/all_gather | solution.py:120
  114.1 3.6 %multiply_convert_fusion.2 = (bf16[768,256]{1,0:T(8,128)(2,1)S(1)}, bf16[768,256]{1,0:T(8,128)(2,1)S(1)}) fusion(f32[768,256]{1,0:T(8,128)S(1)} %fusion.16, f32[768,256]{1,0:T(8,128)} %fusion.19, bf16[768,2048]{1,0:T(8,128)(2,1)} %bitcast.126, bf16[1,256,2048]{2,1,0:T(8,128)(2,1)} %param.24), kind=kOutput, calls=%fused_computation.44 | convolution fusion | flops 807862272 | bytes 6553600 | tf_op jit(solution)/shard_map/erd,efd->erf/dot_general | solution.py:137
  117.7 1.0 fusion.14
  118.8 2.7 add_convert_fusion
  121.6 37.8 %reduce-scatter.3.cloned.1.call-done = bf16[8,96,512]{2,1,0:T(8,128)(2,1)} async-done(((bf16[8,96,2048]{2,1,0:T(8,128)(2,1)}), bf16[8,96,512]{2,1,0:T(8,128)(2,1)}) %reduce-scatter.3.cloned.1.call-update) | async-done | bytes 786448 | tf_op jit(solution)/shard_map/reduce_scatter | solution.py:155
  159.4 25.6 %all_to_all.17 = bf16[8,96,512]{2,1,0:T(8,128)(2,1)} all-to-all(bf16[8,96,512]{2,1,0:T(8,128)(2,1)} %reduce-scatter.3.cloned.1.call-done), channel_id=1, replica_groups=mesh['sp'=8,'tp'=4] {'sp'}, dimensions={0} | all-to-all | bytes 1572864 | tf_op jit(solution)/shard_map/all_to_all | solution.py:159
  185.0 0.2 reduce-scatter.5.cloned.1.call-start
  185.5 0.4 fusion.25
  186.0 0.7 copy-done.11
  187.0 0.1 mul.397
  187.2 0.3 fusion.10
  187.5 0.8 copy.89
  188.3 0.7 slice.217
  188.9 0.7 slice.226
  189.6 0.7 slice.219
  190.3 18.6 %all-gather = f32[8,1,256]{2,1,0:T(1,128)S(1)} all-gather(f32[1,1,256]{2,1,0:T(1,128)S(1)} %reshape.345), channel_id=1, replica_groups=mesh['sp'=8,'tp'=4] {'sp'}, dimensions={0}, use_global_device_ids=true | all-gather | bytes 9216 | tf_op jit(solution)/shard_map/all_gather | solution.py:15
  209.0 0.4 rev.13
  209.4 0.2 fusion.26
  209.8 1.4 rev.14
  211.2 0.6 all-gather.10.cloned.1.call-done
  211.8 6.7 %gather_fusion.2 = bf16[384,2048]{1,0:T(8,128)(2,1)S(1)} fusion(bf16[768,2048]{1,0:T(8,128)(2,1)} %bitcast.99, s32[1024]{0:T(1024)S(1)} %pad_clamp_fusion), kind=kCustom, calls=%fused_computation.2 | custom fusion | bytes 3147264 | tf_op jit(solution)/shard_map/gather | solution.py:161
  218.5 3.4 %reshape.320 = f32[192,2,2048]{2,1,0:T(2,128)} reshape(bf16[384,2048]{1,0:T(8,128)(2,1)S(1)} %gather_fusion.2) | data formatting | bytes 4718592 | tf_op jit(solution)/shard_map/convert_element_type | solution.py:161
  221.8 5.7 %reduce_sum.63 = f32[192,2048]{1,0:T(8,128)S(1)} reduce(f32[192,2,2048]{2,1,0:T(2,128)} %reshape.320, f32[]{:T(128)} %constant.89.clone.1), dimensions={1}, to_apply=%region_7.8 | reduce | flops 393216 | bytes 4718596 | tf_op jit(solution)/shard_map/reduce_sum | solution.py:162
  227.6 0.3 fusion.6
  227.9 0.8 copy-done.4
  228.7 0.5 fusion.5
  229.3 0.4 fusion.47
  230.0 0.2 copy-done.15
  231.8 0.7 fusion.71
  232.5 0.4 rev.12
  232.8 20.5 %all-gather.1 = f32[8,1,256]{2,1,0:T(1,128)S(1)} all-gather(f32[1,1,256]{2,1,0:T(1,128)S(1)} %fusion.71), channel_id=1, replica_groups=mesh['sp'=8,'tp'=4] {'sp'}, dimensions={0}, use_global_device_ids=true | all-gather | bytes 9216 | tf_op jit(solution)/shard_map/all_gather | solution.py:15
  253.4 0.5 while.14
  254.0 1.2 fusion.39
  255.2 1.9 fusion.50
  257.1 4.4 %convolution_bitcast_fusion.2 = f32[1,2048,256]{2,1,0:T(8,128)} fusion(bf16[768,2048]{1,0:T(8,128)(2,1)} %bitcast.123, bf16[768,256]{1,0:T(8,128)(2,1)S(1)} %copy-done.7), kind=kOutput, calls=%fused_computation.14 | convolution fusion | flops 805306368 | bytes 5636096 | tf_op jit(solution)/shard_map/erd,erf->edf/dot_general | solution.py:143
  261.5 2.4 convolution_bitcast_fusion.1
  263.9 0.7 copy-done.34
  264.6 2.4 convolution_bitcast_fusion
  267.1 0.3 fusion.86
  267.5 0.1 copy.96
  267.7 0.3 fusion.85
  268.1 0.7 add_add_fusion
  268.8 53.2 %reduce-scatter.5.cloned.1.call-done = f32[256,256]{1,0:T(8,128)} async-done(((f32[2048,256]{1,0:T(8,128)}), f32[256,256]{1,0:T(8,128)}) %reduce-scatter.5.cloned.1.call-update) | async-done | bytes 262160 | tf_op jit(solution)/shard_map/reduce_scatter | solution.py:182
  (214 shorter events, 3.8 us)
Async XLA Ops:
  7.2 79.4 %copy-start = (bf16[1,2048,256]{2,1,0:T(8,128)(2,1)S(1)}, bf16[1,2048,256]{2,1,0:T(8,128)(2,1)}, u32[]{:S(2)}) copy-start(bf16[1,2048,256]{2,1,0:T(8,128)(2,1)} %param.22) | copy-start | bytes 3145732
  7.2 79.3 %all-gather.6.cloned.1.call-start = ((), (), s32[]{:S(2)}) async-start(), calls=%async_computation.5 | async-start | bytes 3932160 | tf_op jit(solution)/shard_map/all_gather | solution.py:121
  16.9 28.7 %copy-start.3 = (bf16[192,2048]{1,0:T(8,128)(2,1)S(1)}, bf16[192,2048]{1,0:T(8,128)(2,1)}, u32[]{:S(2)}) copy-start(bf16[192,2048]{1,0:T(8,128)(2,1)} %param.17) | copy-start | bytes 2359300
  45.5 68.6 %all-gather.8.cloned.1.call-start = ((), (), s32[]{:S(2)}) async-start(), calls=%async_computation.6 | async-start | bytes 3932160 | tf_op jit(solution)/shard_map/all_gather | solution.py:120
  48.9 5.5 %copy-start.27 = (f32[192,2]{0,1:T(2,128)S(1)}, f32[192,2]{0,1:T(2,128)}, u32[]{:S(2)}) copy-start(f32[192,2]{0,1:T(2,128)} %param.21) | copy-start | bytes 4612
  86.4 73.0 %reduce-scatter.3.cloned.1.call-start = ((), (), s32[]{:S(2)}) async-start(), calls=%async_computation.7 | async-start | bytes 3932160 | tf_op jit(solution)/shard_map/reduce_scatter | solution.py:155
  86.5 3.0 copy-start.9
  86.5 3.2 copy-start.29
  89.7 24.5 %copy-start.32 = (f32[768,256]{1,0:T(8,128)}, f32[768,256]{1,0:T(8,128)S(1)}, u32[]{:S(2)}) copy-start(f32[768,256]{1,0:T(8,128)S(1)} %fusion.16) | copy-start | bytes 2359300
  117.7 1.0 copy-start.6
  117.7 1.0 copy-start.18
  121.5 63.8 %copy-start.13 = (bf16[192,256]{1,0:T(8,128)(2,1)S(1)}, bf16[192,256]{1,0:T(8,128)(2,1)}, u32[]{:S(2)}) copy-start(bf16[192,256]{1,0:T(8,128)(2,1)} %param.26) | copy-start | bytes 294916
  121.5 63.9 %copy-start.28 = (f32[256]{0:T(256)S(1)}, f32[256]{0:T(256)}, u32[]{:S(2)}) copy-start(f32[256]{0:T(256)} %param.29) | copy-start | bytes 3076
  121.5 64.0 %copy-start.24 = (bf16[4,64,64]{2,1,0:T(8,128)(2,1)S(1)}, bf16[4,64,64]{2,1,0:T(8,128)(2,1)}, u32[]{:S(2)}) copy-start(bf16[4,64,64]{2,1,0:T(8,128)(2,1)} %param.30) | copy-start | bytes 98308
  121.6 90.2 %all-gather.10.cloned.1.call-start = ((), (), s32[]{:S(2)}) async-start(), calls=%async_computation.8 | async-start | bytes 3932160 | tf_op jit(solution)/shard_map/all_gather | solution.py:160
  185.0 1.9 copy-start.26
  185.0 2.1 copy-start.22
  185.0 136.9 %reduce-scatter.5.cloned.1.call-start = ((), (), s32[]{:S(2)}) async-start(), calls=%async_computation.9 | async-start | bytes 2359296 | tf_op jit(solution)/shard_map/reduce_scatter | solution.py:182
  186.0 0.7 copy-start.11
  221.8 5.7 %copy-start.2 = (bf16[192,2048]{1,0:T(8,128)(2,1)S(1)}, bf16[192,2048]{1,0:T(8,128)(2,1)}, u32[]{:S(2)}) copy-start(bf16[192,2048]{1,0:T(8,128)(2,1)} %param.18) | copy-start | bytes 2359300
  221.8 5.7 %copy-start.21 = (f32[2048]{0:T(1024)S(1)}, f32[2048]{0:T(1024)}, u32[]{:S(2)}) copy-start(f32[2048]{0:T(1024)} %param.19) | copy-start | bytes 24580
  227.6 1.1 copy-start.4
  227.9 1.4 copy-start.8
  227.9 1.4 copy-start.10
  229.3 0.9 copy-start.15
  229.3 0.9 copy-start.16
  230.2 1.4 copy-start.17
  231.3 22.6 %copy-start.5 = (f32[192,256]{1,0:T(8,128)S(1)}, f32[192,256]{1,0:T(8,128)}, u32[]{:S(2)}) copy-start(f32[192,256]{1,0:T(8,128)} %copy.89) | copy-start | bytes 589828
  231.3 22.6 %copy-start.12 = (f32[192,256]{1,0:T(8,128)S(1)}, f32[192,256]{1,0:T(8,128)}, u32[]{:S(2)}) copy-start(f32[192,256]{1,0:T(8,128)} %rev.14) | copy-start | bytes 589828
  231.3 22.6 %copy-start.14 = (bf16[192,256]{1,0:T(8,128)(2,1)S(1)}, bf16[192,256]{1,0:T(8,128)(2,1)}, u32[]{:S(2)}) copy-start(bf16[192,256]{1,0:T(8,128)(2,1)} %param.26) | copy-start | bytes 294916
  231.3 22.6 %copy-start.20 = (bf16[192,256]{1,0:T(8,128)(2,1)S(1)}, bf16[192,256]{1,0:T(8,128)(2,1)}, u32[]{:S(2)}) copy-start(bf16[192,256]{1,0:T(8,128)(2,1)} %param.28) | copy-start | bytes 294916
  255.2 1.9 copy-start.7
  257.1 4.4 %copy-start.19 = (bf16[768,256]{1,0:T(8,128)(2,1)S(1)}, bf16[768,256]{1,0:T(8,128)(2,1)}, u32[]{:S(2)}) copy-start(bf16[768,256]{1,0:T(8,128)(2,1)} %copy-done.18) | copy-start | bytes 1179652
  257.1 4.4 %copy-start.30 = (bf16[8,96,2048]{2,1,0:T(8,128)(2,1)S(1)}, bf16[8,96,2048]{2,1,0:T(8,128)(2,1)}, u32[]{:S(2)}) copy-start(bf16[8,96,2048]{2,1,0:T(8,128)(2,1)} %all-gather.6.cloned.1.call-done) | copy-start | bytes 9437188
  261.5 2.4 copy-start.31
  261.5 2.4 copy-start.33
  261.5 3.1 copy-start.34
  264.6 2.5 copy-start.23
  264.6 3.1 copy-start.25
  264.6 57.4 %copy-start.1 = (bf16[1,2048,256]{2,1,0:T(8,128)(2,1)S(1)}, bf16[1,2048,256]{2,1,0:T(8,128)(2,1)}, u32[]{:S(2)}) copy-start(bf16[1,2048,256]{2,1,0:T(8,128)(2,1)} %param.22) | copy-start | bytes 3145732
Sparse Core Ops, SparseCore 0:
  45.7 27.5 all-gather.5
  86.6 27.5 all-gather.7
  121.7 37.7 reduce-scatter.2
  185.1 26.5 all-gather.9
  257.2 64.6 reduce-scatter.4
where the time goes:
time: 329 us; the launch traced here: 328 us
  blocking collectives  116 us (35%)
  waiting for transfers between devices  114 us (35%)
  local copies, waits for them, and re-layouts  40.5 us (12%)
  matrix products  24.8 us (8%)
  other arithmetic  17.6 us (5%)
  between operations  14.9 us (5%)
    reduce_scatter x1, waiting for transfers between devices, per_device(): lax.psum_scatter(lax.dot_general(d_mix, branch_out, (((0,), (0,)), ((), (...  53.2 us
    all_gather x2, blocking collectives, entering(): gathered = jax.tree.map(lambda a: lax.all_gather(a, axis), part)  39.1 us
    reduce_scatter x1, waiting for transfers between devices, per_device(): lax.psum_scatter(back_terms, 'tp', scatter_dimension=2, tiled=True)  37.8 us
    all_to_all x1, blocking collectives, per_device(): lax.all_to_all(rows_part, 'sp', split_axis=0, concat_axis=0, tiled=True)  27.3 us
    all_to_all x1, blocking collectives, per_device(): lax.all_to_all(summed, 'sp', split_axis=0, concat_axis=0, tiled=True)  25.6 us
    all_to_all x1, blocking collectives, per_device(): lax.all_to_all(cot_part, 'sp', split_axis=0, concat_axis=0, tiled=True)  23.6 us
    all_gather x1, waiting for transfers between devices, per_device(): lax.all_gather(cot_part, 'tp', axis=2, tiled=True)  22.6 us
    mul x3, local copies, waits for them, and re-layouts, per_device(): route_weights[:, :, None] * cotangent.astype(jnp.float32)[:, None, :]  8.95 us
  transfers between devices with their start and end apart: 5, of which 4 were waited for; matrix products, arithmetic and copies ran while one was open for 12% of the time, Pallas kernels for 0%

commit v1 on v0

v1 whole, which is shorter than its diff:
```python
import functools

import jax
import jax.numpy as jnp
from jax import lax
from jax.sharding import PartitionSpec as P
from jax.experimental import pallas as pl
from jax.experimental.pallas import tpu as pltpu

RATE_SCALE = 8.0
NORM_EPS = 1e-06
SERIES_EDGE = 0.001
MESH = pl.DeviceIdType.MESH


def my_place(tp_count):
    s = lax.axis_index("sp")
    t = lax.axis_index("tp")
    beside = t + 1 - 2 * lax.rem(t, 2)
    across = lax.rem(t + tp_count // 2, tp_count)
    return s, t, beside, across


def greet(sp_count, s, t, beside, across):
    barrier = pltpu.get_barrier_semaphore()
    for other in (beside, across):
        pl.semaphore_signal(barrier, inc=1, device_id=(s, other), device_id_type=MESH)

    def one(i, carry):
        pl.semaphore_signal(
            barrier, inc=1, device_id=(lax.rem(s + i, sp_count), t), device_id_type=MESH
        )
        return carry

    lax.fori_loop(1, sp_count, one, 0)
    pl.semaphore_wait(barrier, sp_count + 1)


def remote(src, dst, send_sem, recv_sem, device):
    return pltpu.make_async_remote_copy(
        src_ref=src,
        dst_ref=dst,
        send_sem=send_sem,
        recv_sem=recv_sem,
        device_id=device,
        device_id_type=MESH,
    )


def spread_kernel(sp_count, tp_count, count, by_cols, has_small, *refs):
    sends = refs[:count]
    refs = refs[count:]
    if has_small:
        small, refs = refs[0], refs[1:]
    outs = refs[:count]
    refs = refs[count:]
    if has_small:
        small_out, refs = refs[0], refs[1:]
    local_sem, send_sem, recv_sem = refs[:3]
    s, t, beside, across = my_place(tp_count)
    facing = lax.rem(beside + tp_count // 2, tp_count)

    def view(a, source, q):
        rows, cols = sends[a].shape[1:]
        if by_cols:
            return outs[a].at[source, :, pl.ds(pl.multiple_of(q * cols, cols), cols)]
        return outs[a].at[source, pl.ds(pl.multiple_of(q * rows, rows), rows), :]

    def first(a, i):
        target = lax.rem(s + i, sp_count)
        return remote(
            sends[a].at[target],
            view(a, s, t),
            send_sem.at[0, a, i],
            recv_sem.at[0, a, i],
            (target, t),
        )

    def passed(kind, a, i, q, to):
        source = lax.rem(s + sp_count - i, sp_count)
        block = view(a, source, q)
        return remote(block, block, send_sem.at[kind, a, i], recv_sem.at[kind, a, i], (s, to))

    def little(i):
        small_send, small_recv = refs[4:6]
        return remote(
            small,
            small_out.at[s],
            small_send.at[i],
            small_recv.at[i],
            (lax.rem(s + i, sp_count), t),
        )

    greet(sp_count, s, t, beside, across)
    if has_small:
        own_small = pltpu.make_async_copy(small, small_out.at[s], refs[3].at[0])
        own_small.start()

        def start_little(i, carry):
            little(i).start()
            return carry

        lax.fori_loop(1, sp_count, start_little, 0)
    own = [
        pltpu.make_async_copy(sends[a].at[s], view(a, s, t), local_sem.at[a])
        for a in range(count)
    ]
    for copy in own:
        copy.start()

    def start_first(i, carry):
        for a in range(count):
            first(a, i).start()
        return carry

    lax.fori_loop(1, sp_count, start_first, 0)

    def pass_on(i):
        for a in range(count):
            passed(1, a, i, t, across).start()
            passed(2, a, i, t, beside).start()

    def pass_back(i):
        for a in range(count):
            passed(1, a, i, across, across).wait_recv()
            passed(3, a, i, across, beside).start()

    for copy in own:
        copy.wait()
    pass_on(0)

    def landed(i):
        for a in range(count):
            source = lax.rem(s + sp_count - i, sp_count)
            remote(
                sends[a].at[source],
                view(a, source, t),
                send_sem.at[0, a, i],
                recv_sem.at[0, a, i],
                (source, t),
            ).wait_recv()

    landed(1)
    pass_on(1)

    def middle(i, carry):
        landed(i)
        pass_on(i)
        pass_back(i - 2)
        return carry

    lax.fori_loop(2, sp_count, middle, 0)
    pass_back(sp_count - 2)
    pass_back(sp_count - 1)

    def finish(i, carry):
        for a in range(count):
            passed(2, a, i, beside, beside).wait_recv()
            passed(3, a, i, facing, beside).wait_recv()
            passed(1, a, i, t, across).wait_send()
            passed(2, a, i, t, beside).wait_send()
            passed(3, a, i, across, beside).wait_send()
        return carry

    lax.fori_loop(0, sp_count, finish, 0)

    def finish_first(i, carry):
        for a in range(count):
            first(a, i).wait_send()
        if has_small:
            little(i).wait()
        return carry

    lax.fori_loop(1, sp_count, finish_first, 0)
    if has_small:
        own_small.wait()


def spread(sp_count, tp_count, sends, by_cols, small, number):
    outs = []
    for a in sends:
        _, rows, cols = a.shape
        shape = (sp_count, rows, tp_count * cols) if by_cols else (sp_count, tp_count * rows, cols)
        outs.append(jax.ShapeDtypeStruct(shape, a.dtype))
    count = len(sends)
    operands = list(sends)
    sems = [
        pltpu.SemaphoreType.DMA((count,)),
        pltpu.SemaphoreType.DMA((4, count, sp_count)),
        pltpu.SemaphoreType.DMA((4, count, sp_count)),
    ]
    if small is not None:
        operands.append(small)
        outs.append(jax.ShapeDtypeStruct((sp_count,) + small.shape, small.dtype))
        sems += [
            pltpu.SemaphoreType.DMA((1,)),
            pltpu.SemaphoreType.DMA((sp_count,)),
            pltpu.SemaphoreType.DMA((sp_count,)),
        ]
    body = functools.partial(spread_kernel, sp_count, tp_count, count, by_cols, small is not None)
    return pl.pallas_call(
        body,
        out_shape=outs,
        in_specs=[pl.BlockSpec(memory_space=pl.ANY)] * len(operands),
        out_specs=[pl.BlockSpec(memory_space=pl.ANY)] * len(outs),
        scratch_shapes=sems,
        compiler_params=pltpu.CompilerParams(collective_id=number, has_side_effects=True),
        cost_estimate=pl.CostEstimate(flops=0, bytes_accessed=40_000_000, transcendentals=0),
    )(*operands)


def return_kernel(
    sp_count,
    tp_count,
    part,
    pick,
    branch,
    full,
    branch_all,
    from_beside,
    to_across,
    from_across,
    mine,
    leaving,
    arrived,
    quarter,
    send_sem,
    recv_sem,
    branch_send,
    branch_recv,
    last_send,
    last_recv,
    local_sem,
):
    s, t, beside, across = my_place(tp_count)
    facing = lax.rem(beside + tp_count // 2, tp_count)
    width = quarter.shape[1]
    half = sp_count // 2
    s_twin = s + 1 - 2 * lax.rem(s, 2)

    def cols(q):
        return pl.ds(pl.multiple_of(q * width, width), width)

    def place(i):
        return lax.rem(s + i + 1, sp_count)

    def to_beside(i, k):
        q = beside if k == 0 else facing
        return remote(
            part.at[place(i), :, cols(q)],
            from_beside.at[k, place(i)],
            send_sem.at[k, i],
            recv_sem.at[k, i],
            (s, beside),
        )

    def crossing(i):
        return remote(
            to_across.at[place(i)],
            from_across.at[place(i)],
            send_sem.at[2, i],
            recv_sem.at[2, i],
            (s, across),
        )

    def homeward(i):
        return remote(
            leaving.at[place(i)],
            arrived.at[s],
            send_sem.at[3, i],
            recv_sem.at[3, i],
            (place(i), t),
        )

    def branch_out_copy(j):
        return remote(
            branch,
            branch_all.at[s],
            branch_send.at[0, j],
            branch_recv.at[0, j],
            (lax.rem(s + 2 * j, sp_count), t),
        )

    def branch_twin(j):
        block = branch_all.at[lax.rem(s + sp_count - 2 * j, sp_count)]
        return remote(block, block, branch_send.at[1, j], branch_recv.at[1, j], (s_twin, t))

    greet(sp_count, s, t, beside, across)

    def start_beside(i, carry):
        to_beside(i, 1).start()
        to_beside(i, 0).start()
        return carry

    lax.fori_loop(0, sp_count, start_beside, 0)
    own_branch = pltpu.make_async_copy(branch, branch_all.at[s], local_sem.at[0])
    own_branch.start()

    def start_branch(j, carry):
        branch_out_copy(j).start()
        return carry

    lax.fori_loop(1, half, start_branch, 0)

    def cross(i):
        to_beside(i, 1).wait_recv()
        at = place(i)
        total = part[at, :, cols(across)].astype(jnp.float32) + from_beside[1, at].astype(
            jnp.float32
        )
        to_across[at] = total.astype(jnp.bfloat16)
        crossing(i).start()
        to_beside(i, 0).wait_recv()
        mine[at] = part[at, :, cols(t)].astype(jnp.float32) + from_beside[0, at].astype(
            jnp.float32
        )

    def total_of(i):
        crossing(i).wait_recv()
        at = place(i)
        return (mine[at] + from_across[at].astype(jnp.float32)).astype(jnp.bfloat16)

    def leave(i):
        leaving[place(i)] = total_of(i)
        homeward(i).start()

    cross(0)
    cross(1)

    def middle(i, carry):
        cross(i)
        leave(i - 2)
        return carry

    lax.fori_loop(2, sp_count, middle, 0)
    own_branch.wait()
    branch_twin(0).start()
    leave(sp_count - 2)
    arrived[s] = total_of(sp_count - 1)

    def pass_branch(j, carry):
        branch_out_copy(j).wait_recv()
        branch_twin(j).start()
        return carry

    lax.fori_loop(1, half, pass_branch, 0)

    quarter_sum = jnp.dot(pick[s], arrived[s], preferred_element_type=jnp.float32)

    def add_in(i, total):
        source = lax.rem(s + 2 * sp_count - i - 1, sp_count)
        remote(
            leaving.at[source],
            arrived.at[source],
            send_sem.at[3, i],
            recv_sem.at[3, i],
            (source, t),
        ).wait_recv()
        return total + jnp.dot(pick[source], arrived[source], preferred_element_type=jnp.float32)

    quarter_sum = lax.fori_loop(0, sp_count - 1, add_in, quarter_sum)
    quarter[...] = quarter_sum.astype(jnp.bfloat16)

    def gathered(kind, source, q, to):
        return remote(
            source, full.at[:, cols(q)], last_send.at[kind], last_recv.at[kind], (s, to)
        )

    own_quarter = pltpu.make_async_copy(quarter, full.at[:, cols(t)], local_sem.at[1])
    gathered(0, quarter, t, across).start()
    gathered(1, quarter, t, beside).start()
    own_quarter.start()
    gathered(0, quarter, across, across).wait_recv()
    gathered(2, full.at[:, cols(across)], across, beside).start()

    def finish(i, carry):
        to_beside(i, 0).wait_send()
        to_beside(i, 1).wait_send()
        crossing(i).wait_send()
        return carry

    lax.fori_loop(0, sp_count, finish, 0)

    def finish_home(i, carry):
        homeward(i).wait_send()
        return carry

    lax.fori_loop(0, sp_count - 1, finish_home, 0)

    def finish_branch(j, carry):
        branch_out_copy(j).wait_send()
        branch_twin(j).wait()
        return carry

    lax.fori_loop(1, half, finish_branch, 0)
    branch_twin(0).wait()
    own_quarter.wait()
    gathered(1, quarter, beside, beside).wait_recv()
    gathered(2, full.at[:, cols(facing)], facing, beside).wait_recv()
    gathered(0, quarter, t, across).wait_send()
    gathered(1, quarter, t, beside).wait_send()
    gathered(2, full.at[:, cols(across)], across, beside).wait_send()


def give_back(sp_count, tp_count, part, pick, branch, number):
    cap, model_width = part.shape[1:]
    width = model_width // tp_count
    rows = branch.shape[0]
    blocks = (sp_count, cap, width)
    return pl.pallas_call(
        functools.partial(return_kernel, sp_count, tp_count),
        out_shape=[
            jax.ShapeDtypeStruct((rows, model_width), jnp.bfloat16),
            jax.ShapeDtypeStruct((sp_count,) + branch.shape, branch.dtype),
        ],
        in_specs=[
            pl.BlockSpec(memory_space=pltpu.VMEM),
            pl.BlockSpec(memory_space=pltpu.VMEM),
            pl.BlockSpec(memory_space=pl.ANY),
        ],
        out_specs=[pl.BlockSpec(memory_space=pl.ANY)] * 2,
        scratch_shapes=[
            pltpu.VMEM((2,) + blocks, jnp.bfloat16),
            pltpu.VMEM(blocks, jnp.bfloat16),
            pltpu.VMEM(blocks, jnp.bfloat16),
            pltpu.VMEM(blocks, jnp.float32),
            pltpu.VMEM(blocks, jnp.bfloat16),
            pltpu.VMEM(blocks, jnp.bfloat16),
            pltpu.VMEM((rows, width), jnp.bfloat16),
            pltpu.SemaphoreType.DMA((4, sp_count)),
            pltpu.SemaphoreType.DMA((4, sp_count)),
            pltpu.SemaphoreType.DMA((2, sp_count // 2)),
            pltpu.SemaphoreType.DMA((2, sp_count // 2)),
            pltpu.SemaphoreType.DMA((3,)),
            pltpu.SemaphoreType.DMA((3,)),
            pltpu.SemaphoreType.DMA((2,)),
        ],
        compiler_params=pltpu.CompilerParams(collective_id=number, has_side_effects=True),
        cost_estimate=pl.CostEstimate(flops=0, bytes_accessed=40_000_000, transcendentals=0),
    )(part, pick, branch)


def gelu_pair(values):
    result, pullback = jax.vjp(jax.nn.gelu, values)
    return (result, pullback(jnp.ones_like(values))[0])


def gate_maps(conv_out, weights):
    rows_here = conv_out.shape[0]
    blocked = conv_out.reshape(rows_here, weights.shape[0], weights.shape[1])
    mapped = jnp.einsum("tbi,bij->tbj", blocked, weights, preferred_element_type=jnp.float32)
    return mapped.reshape(rows_here, -1)


def gate_maps_back(grad_values, weights):
    rows_here = grad_values.shape[0]
    blocked = grad_values.reshape(rows_here, weights.shape[0], weights.shape[2])
    mapped = jnp.einsum(
        "tbj,bij->tbi", blocked, weights.astype(jnp.float32), precision=lax.Precision.HIGHEST
    )
    return mapped.reshape(rows_here, -1)


def norm_slope(spread):
    tiny_side = spread < SERIES_EDGE
    denominator = jnp.where(tiny_side, 1.0, -jnp.expm1(-spread))
    series_ratio = jnp.where(tiny_side, 1.0 + 0.5 * spread, spread / denominator)
    return 0.5 * jnp.sqrt(spread * series_ratio)


def reverse_linear(factors, term_values):

    def combine(left_pair, right_pair):
        return (left_pair[0] * right_pair[0], right_pair[0] * left_pair[1] + right_pair[1])

    flipped = lax.associative_scan(
        combine, (jnp.flip(factors, 0), jnp.flip(term_values, 0)), axis=0
    )
    return jnp.flip(flipped[1], 0)


def per_device(
    cotangent,
    residual,
    norm_gain,
    route_ids,
    route_weights,
    expert_gate,
    expert_up,
    expert_down,
    out_proj,
    conv_out,
    branch_gate,
    prev_state,
    decay_param,
    rate_map,
    input_map,
):
    tok_rows, model_width = residual.shape
    sp_count = lax.axis_size("sp")
    tp_count = lax.axis_size("tp")
    experts_all = expert_gate.shape[0] * sp_count
    capacity = 4 * tok_rows // experts_all
    slot_total = experts_all * capacity
    part_cols = model_width // tp_count
    col_start = lax.axis_index("tp") * part_cols
    res_values = residual.astype(jnp.float32)
    inv_rms = lax.rsqrt(jnp.mean(res_values * res_values, axis=1, keepdims=True) + NORM_EPS)

    def my_cols(values):
        return lax.dynamic_slice_in_dim(values, col_start, part_cols, values.ndim - 1)

    moe_part = (
        my_cols(residual).astype(jnp.float32) * inv_rms * my_cols(norm_gain)[None, :]
    ).astype(jnp.bfloat16)
    flat_ids = route_ids.reshape(-1)
    expert_hits = (flat_ids[:, None] == jnp.arange(experts_all, dtype=jnp.int32)[None, :]).astype(
        jnp.int32
    )
    earlier_hits = jnp.cumsum(expert_hits, axis=0) - expert_hits
    slot_pos = flat_ids * capacity + jnp.sum(earlier_hits * expert_hits, axis=1)
    slot_pair = slot_pos.reshape(tok_rows, 2)
    slots = jnp.arange(slot_total, dtype=jnp.int32)
    hit_first = slots[:, None] == slot_pair[None, :, 0]
    hit_second = slots[:, None] == slot_pair[None, :, 1]
    slot_weight = jnp.sum(
        jnp.where(hit_first, route_weights[None, :, 0], 0.0)
        + jnp.where(hit_second, route_weights[None, :, 1], 0.0),
        axis=1,
        keepdims=True,
    )
    choose = (hit_first | hit_second).astype(jnp.bfloat16)
    rows_part = jnp.dot(choose, moe_part, preferred_element_type=jnp.float32).astype(jnp.bfloat16)
    cot_part = (
        jnp.dot(choose, my_cols(cotangent), preferred_element_type=jnp.float32) * slot_weight
    ).astype(jnp.bfloat16)
    block_rows = slot_total // sp_count
    rows_in, cot_in = spread(
        sp_count,
        tp_count,
        (
            rows_part.reshape(sp_count, block_rows, part_cols),
            cot_part.reshape(sp_count, block_rows, part_cols),
        ),
        True,
        None,
        1,
    )
    rows_in = rows_in.reshape(slot_total, model_width)
    cot_in = cot_in.reshape(slot_total, model_width)
    gate_w, up_w, down_w = expert_gate[0], expert_up[0], expert_down[0]
    gate_pre = jnp.dot(rows_in, gate_w, preferred_element_type=jnp.float32)
    up_pre = jnp.dot(rows_in, up_w, preferred_element_type=jnp.float32)
    gate_sig = jax.nn.sigmoid(gate_pre)
    gate_act = gate_pre * gate_sig
    hidden = (gate_act * up_pre).astype(jnp.bfloat16)
    d_hidden = jnp.einsum("rd,fd->rf", cot_in, down_w, preferred_element_type=jnp.float32)
    d_up = (d_hidden * gate_act).astype(jnp.bfloat16)
    d_gate = (d_hidden * up_pre * gate_sig * (1.0 + gate_pre * (1.0 - gate_sig))).astype(
        jnp.bfloat16
    )
    grad_down = jnp.einsum("rf,rd->fd", hidden, cot_in, preferred_element_type=jnp.float32)[None]
    grad_gate = jnp.einsum("rd,rf->df", rows_in, d_gate, preferred_element_type=jnp.float32)[None]
    grad_up = jnp.einsum("rd,rf->df", rows_in, d_up, preferred_element_type=jnp.float32)[None]
    back_terms = jnp.einsum("rf,df->rd", d_gate, gate_w, preferred_element_type=jnp.float32)
    back_terms = back_terms + jnp.einsum("rf,df->rd", d_up, up_w, preferred_element_type=jnp.float32)
    back_terms = back_terms.astype(jnp.bfloat16).reshape(sp_count, block_rows, model_width)
    rate_gate = jax.nn.sigmoid(gate_maps(conv_out, rate_map))
    input_gate = jax.nn.sigmoid(gate_maps(conv_out, input_map))
    soft_decay = jax.nn.softplus(-decay_param)
    log_keep = -RATE_SCALE * rate_gate * soft_decay[None, :]
    keep_rate = jnp.exp(log_keep)
    spread_values = -2.0 * log_keep
    norm_term = jnp.sqrt(-jnp.expm1(-spread_values))
    conv_values = conv_out.astype(jnp.float32)
    prev_values = prev_state.astype(jnp.float32)
    state_now = keep_rate * prev_values + norm_term * input_gate * conv_values
    gelu_value, gelu_slope = gelu_pair(branch_gate.astype(jnp.float32))
    branch_out = (state_now * gelu_value).astype(jnp.bfloat16)
    slot_grid = slots.reshape(sp_count, 1, block_rows)
    pick = (
        (slot_grid == slot_pair[None, :, 0:1]) | (slot_grid == slot_pair[None, :, 1:2])
    ).astype(jnp.bfloat16)
    d_normed, branch_all = give_back(sp_count, tp_count, back_terms, pick, branch_out, 2)
    weighted = norm_gain[None, :] * d_normed.astype(jnp.float32)
    cubed = inv_rms * inv_rms * inv_rms
    d_mix = (
        cotangent.astype(jnp.float32)
        + inv_rms * weighted
        - res_values * cubed * jnp.mean(res_values * weighted, axis=1, keepdims=True)
    ).astype(jnp.bfloat16)
    d_branch = jnp.dot(d_mix, out_proj, preferred_element_type=jnp.float32)
    next_keep = jnp.concatenate([keep_rate[1:], jnp.zeros_like(keep_rate[:1])], axis=0)
    local_grad = reverse_linear(next_keep, d_branch * gelu_value)
    next_log = jnp.concatenate([log_keep[1:], jnp.zeros_like(log_keep[:1])], axis=0)
    tail_keep = jnp.exp(jnp.flip(jnp.cumsum(jnp.flip(next_log, 0), axis=0), 0))
    block_keep = jnp.exp(jnp.sum(log_keep, axis=0))
    head_term = keep_rate[0] * local_grad[0]
    channels = block_keep.shape[0]
    small = jnp.concatenate(
        [block_keep[None], head_term[None], jnp.zeros((6, channels), jnp.float32)], axis=0
    )
    share_rows = tok_rows // tp_count
    out_rows = model_width // sp_count
    mix_share = lax.dynamic_slice_in_dim(d_mix, lax.axis_index("tp") * share_rows, share_rows, 0)
    mix_share = jnp.transpose(mix_share.reshape(share_rows, sp_count, out_rows), (1, 0, 2))
    mix_cols, small_all = spread(sp_count, tp_count, (mix_share,), False, small, 3)
    grad_out_proj = lax.dot_general(
        mix_cols.reshape(sp_count * tok_rows, out_rows),
        branch_all.reshape(sp_count * tok_rows, channels),
        (((0,), (0,)), ((), ())),
        preferred_element_type=jnp.float32,
    )
    place = lax.axis_index("sp")
    carried = jnp.zeros((channels,), jnp.float32)
    for source in range(sp_count - 1, 0, -1):
        carried = jnp.where(
            source > place, small_all[source, 1] + small_all[source, 0] * carried, carried
        )
    state_grad = local_grad + tail_keep * carried[None, :]
    grad_branch_gate = d_branch * state_now * gelu_slope
    keep_grad = state_grad * prev_values * keep_rate
    inner_input = input_gate * conv_values
    rate_back = keep_grad * (-RATE_SCALE * soft_decay[None, :]) * rate_gate * (1.0 - rate_gate)
    rate_back = rate_back + state_grad * inner_input * keep_rate * keep_rate * (
        1.0 - rate_gate
    ) * norm_slope(spread_values)
    input_back = state_grad * norm_term * conv_values * input_gate * (1.0 - input_gate)
    grad_conv_out = (
        state_grad * norm_term * input_gate
        + gate_maps_back(rate_back, rate_map)
        + gate_maps_back(input_back, input_map)
    )
    return (grad_gate, grad_up, grad_down, grad_out_proj, grad_conv_out, grad_branch_gate)


def solution(mesh):
    in_specs = (
        P("sp", None),
        P("sp", None),
        P(),
        P("sp", None),
        P("sp", None),
        P("sp", None, "tp"),
        P("sp", None, "tp"),
        P("sp", "tp", None),
        P(None, "tp"),
        P("sp", "tp"),
        P("sp", "tp"),
        P("sp", "tp"),
        P("tp"),
        P("tp", None, None),
        P("tp", None, None),
    )
    out_specs = (
        P("sp", None, "tp"),
        P("sp", None, "tp"),
        P("sp", "tp", None),
        P("sp", "tp"),
        P("sp", "tp"),
        P("sp", "tp"),
    )
    return jax.shard_map(
        per_device, mesh=mesh, in_specs=in_specs, out_specs=out_specs, check_vma=False
    )
```

time: 329 us -> 169 us (0.51)
  Pallas kernels: 0 us -> 121 us
  blocking collectives: 116 us -> 0 us
  waiting for transfers between devices: 114 us -> 0 us
  local copies, waits for them, and re-layouts: 40.5 us -> 8.28 us
  between operations: 14.9 us -> 1.58 us
  other arithmetic: 17.6 us -> 10.7 us
    pallas_call x0 -> x3, Pallas kernels: none -> 121 us  [the longest x2 76.7 us: spread(): pl.pallas_call(body, out_shape=outs, in_specs=[pl.BlockSpec(memory_space=...]
    reduce_scatter x2 -> x0, waiting for transfers between devices: 91 us -> none  [the longest x1 53.2 us: per_device(): lax.psum_scatter(lax.dot_general(d_mix, branch_out, (((0,), (0,)), ((), (...]
    all_to_all x3 -> x0, blocking collectives: 76.5 us -> none  [the longest x1 27.3 us: per_device(): lax.all_to_all(rows_part, 'sp', split_axis=0, concat_axis=0, tiled=True)]
    all_gather x2 -> x0, blocking collectives: 39.1 us -> none  [entering(): gathered = jax.tree.map(lambda a: lax.all_gather(a, axis), part)]
    all_gather x3 -> x0, waiting for transfers between devices: 23.2 us -> none  [the longest x1 22.6 us: per_device(): lax.all_gather(cot_part, 'tp', axis=2, tiled=True)]
    gather x3 -> x0, local copies, waits for them, and re-layouts: 15.2 us -> none  [the longest x1 6.69 us: per_device(): returned.reshape(slot_total, model_width)[slot_pos].astype(jnp.float32)]
    mul x5 -> x0, local copies, waits for them, and re-layouts: 9.21 us -> none  [the longest x3 8.95 us: per_device(): route_weights[:, :, None] * cotangent.astype(jnp.float32)[:, None, :]]
    reduce_sum x2 -> x1, other arithmetic: 5.9 us -> 0.19 us  [per_device(): jnp.sum(jnp.where(hit_first, route_weights[None, :, 0], 0.0) + jnp.where(...]
  transfers between devices with their start and end apart: 5 -> 0, of which waited for: 4 -> 0; matrix products, arithmetic and copies ran while one was open for 12% -> 0% of each run, Pallas kernels for 0% -> 0%
where the time goes in v1:
time: 169 us
  Pallas kernels  121 us (72%)
  matrix products  26.8 us (16%)
  other arithmetic  10.7 us (6%)
  local copies, waits for them, and re-layouts  8.28 us (5%)
    pallas_call x2, Pallas kernels, spread(): pl.pallas_call(body, out_shape=outs, in_specs=[pl.BlockSpec(memory_space=...  76.7 us
    pallas_call x1, Pallas kernels, give_back(): pl.pallas_call(functools.partial(return_kernel, sp_count, tp_count), out_...  44.8 us

profile of v1, /device:TPU:0, one launch (start us, length us, event | category | flops | bytes accessed | tf_op | source)
XLA Modules:
  0.0 168.8 jit_solution(9508908253517263325)
XLA Ops:
  0.6 0.0 copy-start
  0.7 0.9 copy.99
  1.5 0.1 eq.86
  1.7 0.9 reduce-window.14
  2.6 0.2 slice_reduce_fusion
  2.8 0.1 eq.82
  3.0 0.1 fusion.64
  3.1 0.1 reduce_sum.48
  3.2 0.1 copy.101
  3.3 0.7 multiply_add_fusion.8
  4.0 0.8 dynamic_slice.13
  4.8 1.4 fusion
  6.1 2.4 %convolution_convert_fusion = bf16[768,512]{1,0:T(8,128)(2,1)} fusion(s32[192]{0:T(256)S(1)} %bitcast.134, s32[192]{0:T(256)S(1)} %bitcast.130, f32[512]{0:T(512)S(1)} %dynamic_slice.13, f32[192]{0:T(256)S(1)} %get-tuple-element.64, bf16[192,2048]{1,0:T(8,128)(2,1)} %param.16, s32[]{:T(128)S(6)} %select_n.102), kind=kOutput, calls=%fused_computation.14 | convolution fusion | flops 152223744 | bytes 987396 | tf_op jit(solution)/shard_map/dot_general | solution.py:533
  8.5 0.2 add_reduce_fusion
  8.7 2.4 %multiply_convert_fusion = bf16[768,512]{1,0:T(8,128)(2,1)} fusion(f32[768]{0:T(1024)S(1)} %add_reduce_fusion, s32[192]{0:T(256)S(1)} %bitcast.136, s32[192]{0:T(256)S(1)} %bitcast.132, bf16[192,2048]{1,0:T(8,128)(2,1)} %param.15, s32[]{:T(128)S(6)} %select_n.102), kind=kOutput, calls=%fused_computation.13 | convolution fusion | flops 152223744 | bytes 987652 | tf_op jit(solution)/shard_map/dot_general | solution.py:535
  11.1 54.3 %shard_map.190 = (bf16[8,96,2048]{2,1,0:T(8,128)(2,1)}, bf16[8,96,2048]{2,1,0:T(8,128)(2,1)}) custom-call(bf16[8,96,512]{2,1,0:T(8,128)(2,1)} %bitcast.120, bf16[8,96,512]{2,1,0:T(8,128)(2,1)} %bitcast.121), custom_call_target="tpu_custom_call" | custom-call | bytes 40000000 | tf_op jit(solution)/shard_map/pallas_call | solution.py:201
  65.4 3.0 %fusion.13 = f32[768,256]{1,0:T(8,128)S(1)} fusion(bf16[768,2048]{1,0:T(8,128)(2,1)} %bitcast.156, bf16[1,2048,256]{2,1,0:T(8,128)(2,1)S(1)} %copy-done), kind=kOutput, calls=%fused_computation.26 | convolution fusion | flops 805306368 | bytes 4980736 | tf_op jit(solution)/shard_map/dot_general | solution.py:552
  68.4 0.1 copy-done.17
  68.5 1.0 fusion.16
  69.5 0.9 copy-done.16
  70.4 0.3 copy-done.18
  70.7 1.2 multiply_convert_fusion.2
  71.9 2.4 %convolution_bitcast_fusion.2 = f32[1,2048,256]{2,1,0:T(8,128)} fusion(bf16[768,2048]{1,0:T(8,128)(2,1)S(1)} %bitcast.158, bf16[768,256]{1,0:T(8,128)(2,1)S(1)} %get-tuple-element.25), kind=kOutput, calls=%fused_computation.3 | convolution fusion | flops 805306368 | bytes 5636096 | tf_op jit(solution)/shard_map/rd,rf->df/dot_general | solution.py:563
  74.3 2.4 %convolution_bitcast_fusion.1 = f32[1,2048,256]{2,1,0:T(8,128)} fusion(bf16[768,2048]{1,0:T(8,128)(2,1)S(1)} %bitcast.159, bf16[768,256]{1,0:T(8,128)(2,1)S(1)} %get-tuple-element.24), kind=kOutput, calls=%fused_computation.2 | convolution fusion | flops 805306368 | bytes 5636096 | tf_op jit(solution)/shard_map/rd,rf->df/dot_general | solution.py:564
  76.7 2.4 %convolution_bitcast_fusion = f32[1,256,2048]{2,1,0:T(8,128)} fusion(bf16[768,2048]{1,0:T(8,128)(2,1)S(1)} %bitcast.155, f32[768,256]{1,0:T(8,128)S(1)} %fusion.16, f32[768,256]{1,0:T(8,128)S(1)} %fusion.13), kind=kOutput, calls=%fused_computation.1 | convolution fusion | flops 806486016 | bytes 6815744 | tf_op jit(solution)/shard_map/rf,rd->fd/dot_general | solution.py:562
  79.1 1.0 fusion.11
  80.1 2.7 %add_convert_fusion = bf16[768,2048]{1,0:T(8,128)(2,1)} fusion(f32[768,2048]{1,0:T(8,128)S(1)} %fusion.11, bf16[768,256]{1,0:T(8,128)(2,1)S(1)} %get-tuple-element.24, bf16[1,2048,256]{2,1,0:T(8,128)(2,1)S(1)} %copy-done.3), kind=kOutput, calls=%fused_computation | convolution fusion | flops 808452096 | bytes 10878976 | tf_op jit(solution)/shard_map/rf,df->rd/dot_general | solution.py:566
  82.8 1.0 or_convert_fusion.pick
  83.8 0.1 mul.433
  83.9 0.1 copy.102
  84.0 0.4 fusion.29
  84.4 0.1 copy.104
  84.5 0.3 fusion.7
  84.8 0.1 copy.106
  84.9 1.0 broadcast_multiply_fusion
  85.9 44.8 %shard_map.191 = (bf16[192,2048]{1,0:T(8,128)(2,1)}, bf16[8,192,256]{2,1,0:T(8,128)(2,1)}) custom-call(bf16[8,96,2048]{2,1,0:T(8,128)(2,1)} %bitcast.111, bf16[8,192,96]{2,1,0:T(8,128)(2,1)} %or_convert_fusion.pick, bf16[192,256]{1,0:T(8,128)(2,1)} %get-tuple-element.31.branch), custom_call_target="tpu_custom_call" | custom-call | bytes 40000000 | tf_op jit(solution)/shard_map/pallas_call | solution.py:410
  130.7 1.6 fusion.4
  132.3 0.6 fusion.3
  132.9 0.7 copy.126
  133.7 0.1 slice.287
  133.8 0.1 slice.280
  133.9 2.4 %fusion.40 = (f32[192,256]{1,0:T(8,128)}, f32[192,256]{1,0:T(8,128)S(1)}) fusion(bf16[192,256]{1,0:T(8,128)(2,1)} %param.25, f32[192,256]{1,0:T(8,128)} %get-tuple-element.32, bf16[192,2048]{1,0:T(8,128)(2,1)S(1)} %fusion.3, bf16[2048,256]{1,0:T(8,128)(2,1)} %param.23), kind=kOutput, calls=%fused_computation.72 | convolution fusion | flops 202407936 | bytes 2523136 | tf_op jit(solution)/shard_map/dot_general | solution.py:592
  136.3 0.1 slice.284
  136.5 0.1 slice.282
  137.8 0.1 slice.334
  138.0 0.1 slice.278
  138.2 0.1 exp.44
  138.3 0.1 pad.65.clone
  138.4 0.7 maximum_maximum_fusion.refs_1_
  139.1 22.4 %shard_map.192 = (bf16[8,192,256]{2,1,0:T(8,128)(2,1)}, f32[8,8,256]{2,1,0:T(8,128)}) custom-call(bf16[8,48,256]{2,1,0:T(8,128)(2,1)} %bitcast.122, f32[8,256]{1,0:T(8,128)} %maximum_maximum_fusion.refs_1_), custom_call_target="tpu_custom_call" | custom-call | bytes 40000000 | tf_op jit(solution)/shard_map/pallas_call | solution.py:201
  161.5 2.5 %convolution_bitcast_fusion.3 = f32[256,256]{1,0:T(8,128)} fusion(bf16[8,192,256]{2,1,0:T(8,128)(2,1)} %get-tuple-element.15, bf16[8,192,256]{2,1,0:T(8,128)(2,1)} %get-tuple-element.16), kind=kOutput, calls=%fused_computation.23 | convolution fusion | flops 201326592 | bytes 1835008 | tf_op jit(solution)/shard_map/dot_general | solution.py:608
  164.0 0.4 rev.12
  164.4 0.9 fusion.77
  165.4 0.4 rev.13
  165.8 0.2 fusion.30
  166.2 0.4 rev.14
  166.6 0.4 fusion.43
  167.0 0.1 copy.118
  167.1 0.3 fusion.86
  167.4 0.1 copy.119
  167.5 0.1 copy.114
  167.7 0.3 fusion.85
  167.9 0.1 copy.115
  168.1 0.7 add_add_fusion
  (141 shorter events, 1.7 us)
Async XLA Ops:
  0.6 64.7 %copy-start = (bf16[1,2048,256]{2,1,0:T(8,128)(2,1)S(1)}, bf16[1,2048,256]{2,1,0:T(8,128)(2,1)}, u32[]{:S(2)}) copy-start(bf16[1,2048,256]{2,1,0:T(8,128)(2,1)} %param.20) | copy-start | bytes 3145732
  0.6 7.9 %copy-start.14 = (f32[192,2]{0,1:T(2,128)S(1)}, f32[192,2]{0,1:T(2,128)}, u32[]{:S(2)}) copy-start(f32[192,2]{0,1:T(2,128)} %param.19) | copy-start | bytes 4612
  65.4 3.1 %copy-start.3 = (bf16[1,2048,256]{2,1,0:T(8,128)(2,1)S(1)}, bf16[1,2048,256]{2,1,0:T(8,128)(2,1)}, u32[]{:S(2)}) copy-start(bf16[1,2048,256]{2,1,0:T(8,128)(2,1)} %param.21) | copy-start | bytes 3145732
  65.4 3.2 %copy-start.17 = (bf16[8,96,2048]{2,1,0:T(8,128)(2,1)S(1)}, bf16[8,96,2048]{2,1,0:T(8,128)(2,1)}, u32[]{:S(2)}) copy-start(bf16[8,96,2048]{2,1,0:T(8,128)(2,1)} %get-tuple-element.12) | copy-start | bytes 9437188
  68.5 1.9 %copy-start.16 = (bf16[8,96,2048]{2,1,0:T(8,128)(2,1)S(1)}, bf16[8,96,2048]{2,1,0:T(8,128)(2,1)}, u32[]{:S(2)}) copy-start(bf16[8,96,2048]{2,1,0:T(8,128)(2,1)} %get-tuple-element.13) | copy-start | bytes 9437188
  68.5 2.2 %copy-start.18 = (bf16[1,256,2048]{2,1,0:T(8,128)(2,1)S(1)}, bf16[1,256,2048]{2,1,0:T(8,128)(2,1)}, u32[]{:S(2)}) copy-start(bf16[1,256,2048]{2,1,0:T(8,128)(2,1)} %param.22) | copy-start | bytes 3145732
  80.1 3.7 %copy-start.15 = (f32[256]{0:T(256)S(1)}, f32[256]{0:T(256)}, u32[]{:S(2)}) copy-start(f32[256]{0:T(256)} %param.27) | copy-start | bytes 3076
  80.1 3.8 %copy-start.4 = (bf16[192,256]{1,0:T(8,128)(2,1)S(1)}, bf16[192,256]{1,0:T(8,128)(2,1)}, u32[]{:S(2)}) copy-start(bf16[192,256]{1,0:T(8,128)(2,1)} %param.24) | copy-start | bytes 294916
  80.1 3.9 %copy-start.11 = (bf16[4,64,64]{2,1,0:T(8,128)(2,1)S(1)}, bf16[4,64,64]{2,1,0:T(8,128)(2,1)}, u32[]{:S(2)}) copy-start(bf16[4,64,64]{2,1,0:T(8,128)(2,1)} %param.28) | copy-start | bytes 98308
  82.8 1.7 copy-start.9
  82.8 2.1 %copy-start.6 = (bf16[192,256]{1,0:T(8,128)(2,1)S(1)}, bf16[192,256]{1,0:T(8,128)(2,1)}, u32[]{:S(2)}) copy-start(bf16[192,256]{1,0:T(8,128)(2,1)} %param.26) | copy-start | bytes 294916
  82.8 2.1 %copy-start.8 = (bf16[192,256]{1,0:T(8,128)(2,1)S(1)}, bf16[192,256]{1,0:T(8,128)(2,1)}, u32[]{:S(2)}) copy-start(bf16[192,256]{1,0:T(8,128)(2,1)} %param.25) | copy-start | bytes 294916
  85.9 44.8 %copy-start.1 = (bf16[192,2048]{1,0:T(8,128)(2,1)S(1)}, bf16[192,2048]{1,0:T(8,128)(2,1)}, u32[]{:S(2)}) copy-start(bf16[192,2048]{1,0:T(8,128)(2,1)} %param.16) | copy-start | bytes 2359300
  85.9 44.8 %copy-start.13 = (f32[2048]{0:T(1024)S(1)}, f32[2048]{0:T(1024)}, u32[]{:S(2)}) copy-start(f32[2048]{0:T(1024)} %param.17) | copy-start | bytes 24580
  130.7 1.6 copy-start.2
  130.7 1.6 copy-start.5
  164.4 2.2 %copy-start.7 = (bf16[192,256]{1,0:T(8,128)(2,1)S(1)}, bf16[192,256]{1,0:T(8,128)(2,1)}, u32[]{:S(2)}) copy-start(bf16[192,256]{1,0:T(8,128)(2,1)} %param.26) | copy-start | bytes 294916
  165.8 1.3 copy-start.10
  166.1 1.5 copy-start.12

commit v2 on v1

--- a/solution.py
+++ b/solution.py
@@ -21,7 +21,7 @@
     return s, t, beside, across
 
 
-def greet(sp_count, s, t, beside, across):
+def hail(sp_count, s, t, beside, across):
     barrier = pltpu.get_barrier_semaphore()
     for other in (beside, across):
         pl.semaphore_signal(barrier, inc=1, device_id=(s, other), device_id_type=MESH)
@@ -33,7 +33,15 @@
         return carry
 
     lax.fori_loop(1, sp_count, one, 0)
-    pl.semaphore_wait(barrier, sp_count + 1)
+
+
+def await_hails(sp_count):
+    pl.semaphore_wait(pltpu.get_barrier_semaphore(), sp_count + 1)
+
+
+def greet(sp_count, s, t, beside, across):
+    hail(sp_count, s, t, beside, across)
+    await_hails(sp_count)
 
 
 def remote(src, dst, send_sem, recv_sem, device):
@@ -47,18 +55,10 @@
     )
 
 
-def spread_kernel(sp_count, tp_count, count, by_cols, has_small, *refs):
-    sends = refs[:count]
-    refs = refs[count:]
-    if has_small:
-        small, refs = refs[0], refs[1:]
-    outs = refs[:count]
-    refs = refs[count:]
-    if has_small:
-        small_out, refs = refs[0], refs[1:]
-    local_sem, send_sem, recv_sem = refs[:3]
+def spreading(sp_count, tp_count, sends, outs, by_cols, local_sem, send_sem, recv_sem):
     s, t, beside, across = my_place(tp_count)
     facing = lax.rem(beside + tp_count // 2, tp_count)
+    count = len(sends)
 
     def view(a, source, q):
         rows, cols = sends[a].shape[1:]
@@ -76,45 +76,14 @@
             (target, t),
         )
 
+    def own(a):
+        return pltpu.make_async_copy(sends[a].at[s], view(a, s, t), local_sem.at[a])
+
     def passed(kind, a, i, q, to):
         source = lax.rem(s + sp_count - i, sp_count)
         block = view(a, source, q)
         return remote(block, block, send_sem.at[kind, a, i], recv_sem.at[kind, a, i], (s, to))
 
-    def little(i):
-        small_send, small_recv = refs[4:6]
-        return remote(
-            small,
-            small_out.at[s],
-            small_send.at[i],
-            small_recv.at[i],
-            (lax.rem(s + i, sp_count), t),
-        )
-
-    greet(sp_count, s, t, beside, across)
-    if has_small:
-        own_small = pltpu.make_async_copy(small, small_out.at[s], refs[3].at[0])
-        own_small.start()
-
-        def start_little(i, carry):
-            little(i).start()
-            return carry
-
-        lax.fori_loop(1, sp_count, start_little, 0)
-    own = [
-        pltpu.make_async_copy(sends[a].at[s], view(a, s, t), local_sem.at[a])
-        for a in range(count)
-    ]
-    for copy in own:
-        copy.start()
-
-    def start_first(i, carry):
-        for a in range(count):
-            first(a, i).start()
-        return carry
-
-    lax.fori_loop(1, sp_count, start_first, 0)
-
     def pass_on(i):
         for a in range(count):
             passed(1, a, i, t, across).start()
@@ -124,10 +93,6 @@
         for a in range(count):
             passed(1, a, i, across, across).wait_recv()
             passed(3, a, i, across, beside).start()
-
-    for copy in own:
-        copy.wait()
-    pass_on(0)
 
     def landed(i):
         for a in range(count):
@@ -140,72 +105,411 @@
                 (source, t),
             ).wait_recv()
 
-    landed(1)
-    pass_on(1)
-
-    def middle(i, carry):
-        landed(i)
-        pass_on(i)
-        pass_back(i - 2)
-        return carry
-
-    lax.fori_loop(2, sp_count, middle, 0)
-    pass_back(sp_count - 2)
-    pass_back(sp_count - 1)
-
-    def finish(i, carry):
+    def start(i):
         for a in range(count):
-            passed(2, a, i, beside, beside).wait_recv()
-            passed(3, a, i, facing, beside).wait_recv()
-            passed(1, a, i, t, across).wait_send()
-            passed(2, a, i, t, beside).wait_send()
-            passed(3, a, i, across, beside).wait_send()
-        return carry
-
-    lax.fori_loop(0, sp_count, finish, 0)
-
-    def finish_first(i, carry):
+            first(a, i).start()
+
+    def start_own():
         for a in range(count):
-            first(a, i).wait_send()
-        if has_small:
-            little(i).wait()
-        return carry
-
-    lax.fori_loop(1, sp_count, finish_first, 0)
-    if has_small:
-        own_small.wait()
-
-
-def spread(sp_count, tp_count, sends, by_cols, small, number):
-    outs = []
-    for a in sends:
-        _, rows, cols = a.shape
-        shape = (sp_count, rows, tp_count * cols) if by_cols else (sp_count, tp_count * rows, cols)
-        outs.append(jax.ShapeDtypeStruct(shape, a.dtype))
-    count = len(sends)
-    operands = list(sends)
-    sems = [
+            own(a).start()
+
+    def pass_own():
+        for a in range(count):
+            own(a).wait()
+        pass_on(0)
+
+    def relay():
+        landed(1)
+        pass_on(1)
+
+        def middle(i, carry):
+            landed(i)
+            pass_on(i)
+            pass_back(i - 2)
+            return carry
+
+        lax.fori_loop(2, sp_count, middle, 0)
+        pass_back(sp_count - 2)
+        pass_back(sp_count - 1)
+
+    def finish():
+        def one(i, carry):
+            for a in range(count):
+                passed(2, a, i, beside, beside).wait_recv()
+                passed(3, a, i, facing, beside).wait_recv()
+                passed(1, a, i, t, across).wait_send()
+                passed(2, a, i, t, beside).wait_send()
+                passed(3, a, i, across, beside).wait_send()
+            return carry
+
+        lax.fori_loop(0, sp_count, one, 0)
+
+        def one_first(i, carry):
+            for a in range(count):
+                first(a, i).wait_send()
+            return carry
+
+        lax.fori_loop(1, sp_count, one_first, 0)
+
+    return start, start_own, pass_own, relay, finish
+
+
+def spread_sems(sp_count, count):
+    return [
         pltpu.SemaphoreType.DMA((count,)),
         pltpu.SemaphoreType.DMA((4, count, sp_count)),
         pltpu.SemaphoreType.DMA((4, count, sp_count)),
     ]
-    if small is not None:
-        operands.append(small)
-        outs.append(jax.ShapeDtypeStruct((sp_count,) + small.shape, small.dtype))
-        sems += [
-            pltpu.SemaphoreType.DMA((1,)),
-            pltpu.SemaphoreType.DMA((sp_count,)),
-            pltpu.SemaphoreType.DMA((sp_count,)),
+
+
+def one_less_exp(spread):
+    small = jnp.minimum(spread, 0.3)
+    series = jnp.full_like(small, 1.0 / 40320.0)
+    for factorial in (5040.0, 720.0, 120.0, 24.0, 6.0, 2.0, 1.0):
+        series = 1.0 / factorial - small * series
+    return jnp.where(spread < 0.3, small * series, 1.0 - jnp.exp(-spread))
+
+
+def dispatch_kernel(
+    sp_count,
+    tp_count,
+    res,
+    cot,
+    gain,
+    ids,
+    weights,
+    conv,
+    gate,
+    prev,
+    soft,
+    maps,
+    rows_out,
+    cot_out,
+    branch_out,
+    rate_factor,
+    input_factor,
+    direct_factor,
+    gate_factor,
+    gelu_out,
+    keep_out,
+    send_rows,
+    send_cot,
+    moe_part,
+    scaled_first,
+    scaled_second,
+    pre_values,
+    local_sem,
+    send_sem,
+    recv_sem,
+):
+    s, t, beside, across = my_place(tp_count)
+    hail(sp_count, s, t, beside, across)
+    start, start_own, pass_own, relay, finish = spreading(
+        sp_count,
+        tp_count,
+        (send_rows, send_cot),
+        (rows_out, cot_out),
+        True,
+        local_sem,
+        send_sem,
+        recv_sem,
+    )
+    tok_rows = res.shape[0]
+    cap, width = send_rows.shape[1:]
+    cols = pl.ds(pl.multiple_of(t * width, width), width)
+    res_all = res[...].astype(jnp.float32)
+    inv_rms = lax.rsqrt(jnp.mean(res_all * res_all, axis=1, keepdims=True) + NORM_EPS)
+    moe_part[...] = (res[:, cols].astype(jnp.float32) * inv_rms * gain[:, cols]).astype(
+        jnp.bfloat16
+    )
+    cot_mine = cot[:, cols].astype(jnp.float32)
+    scaled_first[...] = (weights[:, 0:1] * cot_mine).astype(jnp.bfloat16)
+    scaled_second[...] = (weights[:, 1:2] * cot_mine).astype(jnp.bfloat16)
+    experts = lax.broadcasted_iota(jnp.int32, (tok_rows, sp_count), 1)
+    is_first = ids[:, 0:1] == experts
+    is_second = ids[:, 1:2] == experts
+    hits = (is_first | is_second).astype(jnp.float32).astype(jnp.bfloat16)
+    earlier = (
+        lax.broadcasted_iota(jnp.int32, (tok_rows, tok_rows), 0)
+        > lax.broadcasted_iota(jnp.int32, (tok_rows, tok_rows), 1)
+    )
+    earlier = earlier.astype(jnp.float32).astype(jnp.bfloat16)
+    ranks = jnp.dot(earlier, hits, preferred_element_type=jnp.float32)
+    slot_first = jnp.sum(jnp.where(is_first, ranks, 0.0), axis=1, keepdims=True)
+    slot_second = jnp.sum(jnp.where(is_second, ranks, 0.0), axis=1, keepdims=True)
+    slot_first = slot_first + (ids[:, 0:1] * cap).astype(jnp.float32)
+    slot_second = slot_second + (ids[:, 1:2] * cap).astype(jnp.float32)
+    lanes = lax.broadcasted_iota(jnp.int32, (tok_rows, cap), 1).astype(jnp.float32)
+    over_rows = (((0,), (0,)), ((), ()))
+
+    def fill(target):
+        base = (target * cap).astype(jnp.float32)
+        first = jnp.where(slot_first - base == lanes, 1.0, 0.0)
+        second = jnp.where(slot_second - base == lanes, 1.0, 0.0)
+        send_rows[target] = lax.dot_general(
+            (first + second).astype(jnp.bfloat16),
+            moe_part[...],
+            over_rows,
+            preferred_element_type=jnp.float32,
+        ).astype(jnp.bfloat16)
+        from_first = lax.dot_general(
+            first.astype(jnp.bfloat16),
+            scaled_first[...],
+            over_rows,
+            preferred_element_type=jnp.float32,
+        )
+        from_second = lax.dot_general(
+            second.astype(jnp.bfloat16),
+            scaled_second[...],
+            over_rows,
+            preferred_element_type=jnp.float32,
+        )
+        send_cot[target] = (from_first + from_second).astype(jnp.bfloat16)
+
+    fill(s)
+    await_hails(sp_count)
+    start_own()
+
+    def send_one(i, carry):
+        fill(lax.rem(s + i, sp_count))
+        start(i)
+        return carry
+
+    lax.fori_loop(1, sp_count, send_one, 0)
+    pass_own()
+    channels = conv.shape[1]
+    pre_values[...] = jnp.dot(conv[...], maps[...], preferred_element_type=jnp.float32)
+    step = 16
+
+    def forward(i, carry):
+        rows = pl.ds(pl.multiple_of(i * step, step), step)
+        rate_gate = jax.nn.sigmoid(pre_values[rows, :channels])
+        input_gate = jax.nn.sigmoid(pre_values[rows, channels:])
+        log_keep = -RATE_SCALE * rate_gate * soft[...]
+        keep = jnp.exp(log_keep)
+        spread = -2.0 * log_keep
+        gone = one_less_exp(spread)
+        norm_term = jnp.sqrt(gone)
+        conv_values = conv[rows, :].astype(jnp.float32)
+        prev_values = prev[rows, :].astype(jnp.float32)
+        inner = input_gate * conv_values
+        state_now = keep * prev_values + norm_term * inner
+        v = gate[rows, :].astype(jnp.float32)
+        root = 0.7978845608028654
+        bent = jnp.tanh(root * (v + 0.044715 * v * v * v))
+        gelu_value = 0.5 * v * (1.0 + bent)
+        gelu_slope = 0.5 * (1.0 + bent) + 0.5 * v * (1.0 - bent * bent) * root * (
+            1.0 + 3.0 * 0.044715 * v * v
+        )
+        tiny_side = spread < SERIES_EDGE
+        series = jnp.where(tiny_side, 1.0 + 0.5 * spread, spread / jnp.where(tiny_side, 1.0, gone))
+        slope = 0.5 * jnp.sqrt(spread * series)
+        branch_out[rows, :] = (state_now * gelu_value).astype(jnp.bfloat16)
+        rate_factor[rows, :] = prev_values * keep * (
+            -RATE_SCALE * soft[...]
+        ) * rate_gate * (1.0 - rate_gate) + inner * keep * keep * (1.0 - rate_gate) * slope
+        input_factor[rows, :] = norm_term * conv_values * input_gate * (1.0 - input_gate)
+        direct_factor[rows, :] = norm_term * input_gate
+        gate_factor[rows, :] = state_now * gelu_slope
+        gelu_out[rows, :] = gelu_value
+        keep_out[rows, :] = keep
+        return carry
+
+    lax.fori_loop(0, tok_rows // step, forward, 0)
+    relay()
+    finish()
+
+
+def dispatch(sp_count, tp_count, cap, operands, number):
+    res, conv = operands[0], operands[5]
+    tok_rows, model_width = res.shape
+    width = model_width // tp_count
+    wide = jax.ShapeDtypeStruct((sp_count, cap, model_width), jnp.bfloat16)
+    factor = jax.ShapeDtypeStruct(conv.shape, jnp.float32)
+    vmem = pl.BlockSpec(memory_space=pltpu.VMEM)
+    anywhere = pl.BlockSpec(memory_space=pl.ANY)
+    return pl.pallas_call(
+        functools.partial(dispatch_kernel, sp_count, tp_count),
+        out_shape=[wide, wide, jax.ShapeDtypeStruct(conv.shape, jnp.bfloat16)] + [factor] * 6,
+        in_specs=[vmem] * len(operands),
+        out_specs=[anywhere] * 2 + [vmem] * 7,
+        scratch_shapes=[
+            pltpu.VMEM((sp_count, cap, width), jnp.bfloat16),
+            pltpu.VMEM((sp_count, cap, width), jnp.bfloat16),
+            pltpu.VMEM((tok_rows, width), jnp.bfloat16),
+            pltpu.VMEM((tok_rows, width), jnp.bfloat16),
+            pltpu.VMEM((tok_rows, width), jnp.bfloat16),
+            pltpu.VMEM((tok_rows, 2 * conv.shape[1]), jnp.float32),
         ]
-    body = functools.partial(spread_kernel, sp_count, tp_count, count, by_cols, small is not None)
-    return pl.pallas_call(
-        body,
-        out_shape=outs,
-        in_specs=[pl.BlockSpec(memory_space=pl.ANY)] * len(operands),
-        out_specs=[pl.BlockSpec(memory_space=pl.ANY)] * len(outs),
-        scratch_shapes=sems,
+        + spread_sems(sp_count, 2),
         compiler_params=pltpu.CompilerParams(collective_id=number, has_side_effects=True),
         cost_estimate=pl.CostEstimate(flops=0, bytes_accessed=40_000_000, transcendentals=0),
+    )(*operands)
+
+
+def tail_kernel(
+    sp_count,
+    tp_count,
+    normed,
+    res,
+    cot,
+    gain,
+    proj,
+    maps,
+    rate_factor,
+    input_factor,
+    direct_factor,
+    gate_factor,
+    gelu_values,
+    keep,
+    mix_out,
+    conv_grad,
+    gate_grad,
+    share,
+    mix,
+    small,
+    small_all,
+    local_sem,
+    send_sem,
+    recv_sem,
+    small_send,
+    small_recv,
+):
+    s, t, beside, across = my_place(tp_count)
+    hail(sp_count, s, t, beside, across)
+    start, start_own, pass_own, relay, finish = spreading(
+        sp_count, tp_count, (share,), (mix_out,), False, local_sem, send_sem, recv_sem
+    )
+    tok_rows, model_width = res.shape
+    share_rows, out_rows = share.shape[1:]
+
+    def mix_rows(begin):
+        rows = pl.ds(pl.multiple_of(begin, share_rows), share_rows)
+        values = res[rows, :].astype(jnp.float32)
+        weighted = gain[...] * normed[rows, :].astype(jnp.float32)
+        inv_rms = lax.rsqrt(jnp.mean(values * values, axis=1, keepdims=True) + NORM_EPS)
+        cubed = inv_rms * inv_rms * inv_rms
+        slope = cubed * jnp.mean(values * weighted, axis=1, keepdims=True)
+        return rows, (
+            cot[rows, :].astype(jnp.float32) + inv_rms * weighted - values * slope
+        ).astype(jnp.bfloat16)
+
+    _, own_rows = mix_rows(t * share_rows)
+    for j in range(sp_count):
+        share[j] = own_rows[:, j * out_rows : (j + 1) * out_rows]
+    await_hails(sp_count)
+    start_own()
+
+    def send_one(i, carry):
+        start(i)
+        return carry
+
+    lax.fori_loop(1, sp_count, send_one, 0)
+
+    def fill(k, carry):
+        rows, values = mix_rows(k * share_rows)
+        mix[rows, :] = values
+        return carry
+
+    lax.fori_loop(0, tp_count, fill, 0)
+    pass_own()
+    d_branch = jnp.dot(mix[...], proj[...], preferred_element_type=jnp.float32)
+    gate_grad[...] = d_branch * gate_factor[...]
+    at = lax.broadcasted_iota(jnp.int32, d_branch.shape, 0)
+    grads = d_branch * gelu_values[...]
+    keeps = jnp.where(at < tok_rows - 1, pltpu.roll(keep[...], tok_rows - 1, 0), 1.0)
+    reach = 1
+    while reach < tok_rows:
+        inside = at < tok_rows - reach
+        later_grads = jnp.where(inside, pltpu.roll(grads, tok_rows - reach, 0), 0.0)
+        later_keeps = jnp.where(inside, pltpu.roll(keeps, tok_rows - reach, 0), 1.0)
+        grads = grads + keeps * later_grads
+        keeps = keeps * later_keeps
+        reach *= 2
+    small[...] = jnp.zeros_like(small)
+    small[0:1, :] = keep[0:1, :] * keeps[0:1, :]
+    small[1:2, :] = keep[0:1, :] * grads[0:1, :]
+    small_all[s] = jnp.zeros(small.shape, jnp.float32)
+
+    def carry_to(i):
+        return remote(
+            small,
+            small_all.at[s],
+            small_send.at[i],
+            small_recv.at[i],
+            (lax.rem(s + i, sp_count), t),
+        )
+
+    def send_small(i, carry):
+        carry_to(i).start()
+        return carry
+
+    lax.fori_loop(1, sp_count, send_small, 0)
+    relay()
+
+    def take_small(i, carry):
+        source = lax.rem(s + sp_count - i, sp_count)
+        remote(
+            small, small_all.at[source], small_send.at[i], small_recv.at[i], (source, t)
+        ).wait_recv()
+        return carry
+
+    lax.fori_loop(1, sp_count, take_small, 0)
+
+    def compose(turn, carried):
+        source = sp_count - 1 - turn
+        later = small_all[source]
+        return jnp.where(source > s, later[1:2] + later[0:1] * carried, carried)
+
+    carried = lax.fori_loop(
+        0, sp_count - 1, compose, jnp.zeros((1, d_branch.shape[1]), jnp.float32)
+    )
+    state_grad = grads + keeps * carried
+    back = jnp.concatenate(
+        [state_grad * rate_factor[...], state_grad * input_factor[...]], axis=1
+    )
+    high = back.astype(jnp.bfloat16)
+    low = (back - high.astype(jnp.float32)).astype(jnp.bfloat16)
+    over_cols = (((1,), (1,)), ((), ()))
+    conv_grad[...] = (
+        state_grad * direct_factor[...]
+        + lax.dot_general(high, maps[...], over_cols, preferred_element_type=jnp.float32)
+        + lax.dot_general(low, maps[...], over_cols, preferred_element_type=jnp.float32)
+    )
+    finish()
+
+    def end_small(i, carry):
+        carry_to(i).wait_send()
+        return carry
+
+    lax.fori_loop(1, sp_count, end_small, 0)
+
+
+def tail(sp_count, tp_count, operands, number):
+    res, keep = operands[1], operands[-1]
+    tok_rows, model_width = res.shape
+    share_rows, out_rows = tok_rows // tp_count, model_width // sp_count
+    factor = jax.ShapeDtypeStruct(keep.shape, jnp.float32)
+    vmem = pl.BlockSpec(memory_space=pltpu.VMEM)
+    return pl.pallas_call(
+        functools.partial(tail_kernel, sp_count, tp_count),
+        out_shape=[
+            jax.ShapeDtypeStruct((sp_count, tok_rows, out_rows), jnp.bfloat16),
+            factor,
+            factor,
+        ],
+        in_specs=[vmem] * len(operands),
+        out_specs=[pl.BlockSpec(memory_space=pl.ANY), vmem, vmem],
+        scratch_shapes=[
+            pltpu.VMEM((sp_count, share_rows, out_rows), jnp.bfloat16),
+            pltpu.VMEM((tok_rows, model_width), jnp.bfloat16),
+            pltpu.VMEM((8, keep.shape[1]), jnp.float32),
+            pltpu.VMEM((sp_count, 8, keep.shape[1]), jnp.float32),
+        ]
+        + spread_sems(sp_count, 1)
+        + [pltpu.SemaphoreType.DMA((sp_count,)), pltpu.SemaphoreType.DMA((sp_count,))],
+        compiler_params=pltpu.CompilerParams(collective_id=number, has_side_effects=True),
+        cost_estimate=pl.CostEstimate(flops=0, bytes_accessed=20_000_000, transcendentals=0),
     )(*operands)
 
 
@@ -440,45 +744,6 @@
     )(part, pick, branch)
 
 
-def gelu_pair(values):
-    result, pullback = jax.vjp(jax.nn.gelu, values)
-    return (result, pullback(jnp.ones_like(values))[0])
-
-
-def gate_maps(conv_out, weights):
-    rows_here = conv_out.shape[0]
-    blocked = conv_out.reshape(rows_here, weights.shape[0], weights.shape[1])
-    mapped = jnp.einsum("tbi,bij->tbj", blocked, weights, preferred_element_type=jnp.float32)
-    return mapped.reshape(rows_here, -1)
-
-
-def gate_maps_back(grad_values, weights):
-    rows_here = grad_values.shape[0]
-    blocked = grad_values.reshape(rows_here, weights.shape[0], weights.shape[2])
-    mapped = jnp.einsum(
-        "tbj,bij->tbi", blocked, weights.astype(jnp.float32), precision=lax.Precision.HIGHEST
-    )
-    return mapped.reshape(rows_here, -1)
-
-
-def norm_slope(spread):
-    tiny_side = spread < SERIES_EDGE
-    denominator = jnp.where(tiny_side, 1.0, -jnp.expm1(-spread))
-    series_ratio = jnp.where(tiny_side, 1.0 + 0.5 * spread, spread / denominator)
-    return 0.5 * jnp.sqrt(spread * series_ratio)
-
-
-def reverse_linear(factors, term_values):
-
-    def combine(left_pair, right_pair):
-        return (left_pair[0] * right_pair[0], right_pair[0] * left_pair[1] + right_pair[1])
-
-    flipped = lax.associative_scan(
-        combine, (jnp.flip(factors, 0), jnp.flip(term_values, 0)), axis=0
-    )
-    return jnp.flip(flipped[1], 0)
-
-
 def per_device(
     cotangent,
     residual,
@@ -502,48 +767,34 @@
     experts_all = expert_gate.shape[0] * sp_count
     capacity = 4 * tok_rows // experts_all
     slot_total = experts_all * capacity
-    part_cols = model_width // tp_count
-    col_start = lax.axis_index("tp") * part_cols
-    res_values = residual.astype(jnp.float32)
-    inv_rms = lax.rsqrt(jnp.mean(res_values * res_values, axis=1, keepdims=True) + NORM_EPS)
-
-    def my_cols(values):
-        return lax.dynamic_slice_in_dim(values, col_start, part_cols, values.ndim - 1)
-
-    moe_part = (
-        my_cols(residual).astype(jnp.float32) * inv_rms * my_cols(norm_gain)[None, :]
-    ).astype(jnp.bfloat16)
-    flat_ids = route_ids.reshape(-1)
-    expert_hits = (flat_ids[:, None] == jnp.arange(experts_all, dtype=jnp.int32)[None, :]).astype(
-        jnp.int32
-    )
-    earlier_hits = jnp.cumsum(expert_hits, axis=0) - expert_hits
-    slot_pos = flat_ids * capacity + jnp.sum(earlier_hits * expert_hits, axis=1)
-    slot_pair = slot_pos.reshape(tok_rows, 2)
-    slots = jnp.arange(slot_total, dtype=jnp.int32)
-    hit_first = slots[:, None] == slot_pair[None, :, 0]
-    hit_second = slots[:, None] == slot_pair[None, :, 1]
-    slot_weight = jnp.sum(
-        jnp.where(hit_first, route_weights[None, :, 0], 0.0)
-        + jnp.where(hit_second, route_weights[None, :, 1], 0.0),
-        axis=1,
-        keepdims=True,
-    )
-    choose = (hit_first | hit_second).astype(jnp.bfloat16)
-    rows_part = jnp.dot(choose, moe_part, preferred_element_type=jnp.float32).astype(jnp.bfloat16)
-    cot_part = (
-        jnp.dot(choose, my_cols(cotangent), preferred_element_type=jnp.float32) * slot_weight
-    ).astype(jnp.bfloat16)
     block_rows = slot_total // sp_count
-    rows_in, cot_in = spread(
+    channels = conv_out.shape[1]
+    block_of = jnp.arange(channels, dtype=jnp.int32) // rate_map.shape[1]
+
+    def whole_map(blocks):
+        rows = blocks.reshape(channels, blocks.shape[2])
+        tiled = jnp.tile(rows, (1, blocks.shape[0]))
+        return jnp.where(block_of[:, None] == block_of[None, :], tiled, jnp.zeros((), tiled.dtype))
+
+    maps = jnp.concatenate([whole_map(rate_map), whole_map(input_map)], axis=1)
+    gain_row = norm_gain[None, :]
+    soft_decay = jax.nn.softplus(-decay_param)[None, :]
+    rows_in, cot_in, branch_out, *factors = dispatch(
         sp_count,
         tp_count,
+        block_rows,
         (
-            rows_part.reshape(sp_count, block_rows, part_cols),
-            cot_part.reshape(sp_count, block_rows, part_cols),
+            residual,
+            cotangent,
+            gain_row,
+            route_ids,
+            route_weights,
+            conv_out,
+            branch_gate,
+            prev_state,
+            soft_decay,
+            maps,
         ),
-        True,
-        None,
         1,
     )
     rows_in = rows_in.reshape(slot_total, model_width)
@@ -565,71 +816,36 @@
     back_terms = jnp.einsum("rf,df->rd", d_gate, gate_w, preferred_element_type=jnp.float32)
     back_terms = back_terms + jnp.einsum("rf,df->rd", d_up, up_w, preferred_element_type=jnp.float32)
     back_terms = back_terms.astype(jnp.bfloat16).reshape(sp_count, block_rows, model_width)
-    rate_gate = jax.nn.sigmoid(gate_maps(conv_out, rate_map))
-    input_gate = jax.nn.sigmoid(gate_maps(conv_out, input_map))
-    soft_decay = jax.nn.softplus(-decay_param)
-    log_keep = -RATE_SCALE * rate_gate * soft_decay[None, :]
-    keep_rate = jnp.exp(log_keep)
-    spread_values = -2.0 * log_keep
-    norm_term = jnp.sqrt(-jnp.expm1(-spread_values))
-    conv_values = conv_out.astype(jnp.float32)
-    prev_values = prev_state.astype(jnp.float32)
-    state_now = keep_rate * prev_values + norm_term * input_gate * conv_values
-    gelu_value, gelu_slope = gelu_pair(branch_gate.astype(jnp.float32))
-    branch_out = (state_now * gelu_value).astype(jnp.bfloat16)
+    expert_hits = (
+        route_ids[:, :, None] == jnp.arange(experts_all, dtype=jnp.int32)[None, None, :]
+    ).astype(jnp.float32)
+    token = jnp.arange(tok_rows, dtype=jnp.int32)
+    earlier = (token[:, None] > token[None, :]).astype(jnp.bfloat16)
+    ranks = jnp.dot(
+        earlier,
+        jnp.sum(expert_hits, axis=1).astype(jnp.bfloat16),
+        preferred_element_type=jnp.float32,
+    )
+    slot_pair = route_ids * capacity + jnp.sum(ranks[:, None, :] * expert_hits, axis=2).astype(
+        jnp.int32
+    )
+    slots = jnp.arange(slot_total, dtype=jnp.int32)
     slot_grid = slots.reshape(sp_count, 1, block_rows)
     pick = (
         (slot_grid == slot_pair[None, :, 0:1]) | (slot_grid == slot_pair[None, :, 1:2])
     ).astype(jnp.bfloat16)
     d_normed, branch_all = give_back(sp_count, tp_count, back_terms, pick, branch_out, 2)
-    weighted = norm_gain[None, :] * d_normed.astype(jnp.float32)
-    cubed = inv_rms * inv_rms * inv_rms
-    d_mix = (
-        cotangent.astype(jnp.float32)
-        + inv_rms * weighted
-        - res_values * cubed * jnp.mean(res_values * weighted, axis=1, keepdims=True)
-    ).astype(jnp.bfloat16)
-    d_branch = jnp.dot(d_mix, out_proj, preferred_element_type=jnp.float32)
-    next_keep = jnp.concatenate([keep_rate[1:], jnp.zeros_like(keep_rate[:1])], axis=0)
-    local_grad = reverse_linear(next_keep, d_branch * gelu_value)
-    next_log = jnp.concatenate([log_keep[1:], jnp.zeros_like(log_keep[:1])], axis=0)
-    tail_keep = jnp.exp(jnp.flip(jnp.cumsum(jnp.flip(next_log, 0), axis=0), 0))
-    block_keep = jnp.exp(jnp.sum(log_keep, axis=0))
-    head_term = keep_rate[0] * local_grad[0]
-    channels = block_keep.shape[0]
-    small = jnp.concatenate(
-        [block_keep[None], head_term[None], jnp.zeros((6, channels), jnp.float32)], axis=0
-    )
-    share_rows = tok_rows // tp_count
-    out_rows = model_width // sp_count
-    mix_share = lax.dynamic_slice_in_dim(d_mix, lax.axis_index("tp") * share_rows, share_rows, 0)
-    mix_share = jnp.transpose(mix_share.reshape(share_rows, sp_count, out_rows), (1, 0, 2))
-    mix_cols, small_all = spread(sp_count, tp_count, (mix_share,), False, small, 3)
+    mix_cols, grad_conv_out, grad_branch_gate = tail(
+        sp_count,
+        tp_count,
+        (d_normed, residual, cotangent, gain_row, out_proj, maps, *factors),
+        3,
+    )
     grad_out_proj = lax.dot_general(
-        mix_cols.reshape(sp_count * tok_rows, out_rows),
+        mix_cols.reshape(sp_count * tok_rows, mix_cols.shape[2]),
         branch_all.reshape(sp_count * tok_rows, channels),
         (((0,), (0,)), ((), ())),
         preferred_element_type=jnp.float32,
-    )
-    place = lax.axis_index("sp")
-    carried = jnp.zeros((channels,), jnp.float32)
-    for source in range(sp_count - 1, 0, -1):
-        carried = jnp.where(
-            source > place, small_all[source, 1] + small_all[source, 0] * carried, carried
-        )
-    state_grad = local_grad + tail_keep * carried[None, :]
-    grad_branch_gate = d_branch * state_now * gelu_slope
-    keep_grad = state_grad * prev_values * keep_rate
-    inner_input = input_gate * conv_values
-    rate_back = keep_grad * (-RATE_SCALE * soft_decay[None, :]) * rate_gate * (1.0 - rate_gate)
-    rate_back = rate_back + state_grad * inner_input * keep_rate * keep_rate * (
-        1.0 - rate_gate
-    ) * norm_slope(spread_values)
-    input_back = state_grad * norm_term * conv_values * input_gate * (1.0 - input_gate)
-    grad_conv_out = (
-        state_grad * norm_term * input_gate
-        + gate_maps_back(rate_back, rate_map)
-        + gate_maps_back(input_back, input_map)
     )
     return (grad_gate, grad_up, grad_down, grad_out_proj, grad_conv_out, grad_branch_gate)
 

time: 169 us -> 158 us (0.935)
  matrix products: 26.8 us -> 18.4 us
  other arithmetic: 10.7 us -> 3.11 us
  Pallas kernels: 121 us -> 126 us
    dot_general x8 -> x2, matrix products: 10.7 us -> 2.39 us  [the longest x1 2.24 us: per_device(): lax.dot_general(mix_cols.reshape(sp_count * tok_rows, mix_cols.shape[2]),...]
    pallas_call x2, Pallas kernels: 76.7 us -> 82.3 us  [the longest x1 58.1 us: dispatch(): pl.pallas_call(functools.partial(dispatch_kernel, sp_count, tp_count), ou...]
    unnamed x41 -> x18, local copies, waits for them, and re-layouts: 2.35 us -> 7.5 us
    reduce_sum x4 -> x2, other arithmetic: 3.24 us -> 0.05 us  [the longest x1 0.04 us: per_device(): jnp.sum(ranks[:, None, :] * expert_hits, axis=2).astype(jnp.int32)]
    another operation x4 -> x6, local copies, waits for them, and re-layouts: 0.04 us -> 2.06 us  [whole_map(): tiled = jnp.tile(rows, (1, blocks.shape[0]))]
where the time goes in v2:
time: 158 us
  Pallas kernels  126 us (80%)
  matrix products  18.4 us (12%)
  local copies, waits for them, and re-layouts  9.56 us (6%)
  other arithmetic  3.11 us (2%)
    pallas_call x1, Pallas kernels, dispatch(): pl.pallas_call(functools.partial(dispatch_kernel, sp_count, tp_count), ou...  58.1 us
    pallas_call x1, Pallas kernels, give_back(): pl.pallas_call(functools.partial(return_kernel, sp_count, tp_count), out_...  43.8 us
    pallas_call x1, Pallas kernels, tail(): pl.pallas_call(functools.partial(tail_kernel, sp_count, tp_count), out_sh...  24.2 us
    unnamed x18, local copies, waits for them, and re-layouts  7.5 us

profile of v2, /device:TPU:0, one launch (start us, length us, event | category | flops | bytes accessed | tf_op | source)
XLA Modules:
  0.0 158.0 jit_solution(11981253863248544532)
XLA Ops:
  0.6 0.0 copy-start
  0.6 1.5 copy.37.ids
  2.2 1.4 copy.38.weights
  3.6 1.3 compare_select_fusion.2
  4.9 0.9 copy.33
  5.8 0.1 copy.34
  5.9 0.9 copy.35
  6.9 0.1 copy.36
  7.0 0.1 compare_select_fusion.1
  7.1 0.7 pad_maximum_fusion.maps
  7.8 58.1 %shard_map.190 = (bf16[8,96,2048]{2,1,0:T(8,128)(2,1)}, bf16[8,96,2048]{2,1,0:T(8,128)(2,1)}, bf16[192,256]{1,0:T(8,128)(2,1)}, f32[192,256]{1,0:T(8,128)}, f32[...) custom-call(bf16[192,2048]{1,0:T(8,128)(2,1)} %res.3, ...), custom_call_target="tpu_custom_call" | custom-call | bytes 40000000 | tf_op jit(solution)/shard_map/pallas_call | solution.py:331
  65.9 0.0 copy-start.1
  65.9 0.0 copy-start.4
  65.9 0.0 copy-done
  65.9 3.0 %fusion.2 = f32[768,256]{1,0:T(8,128)S(1)} fusion(bf16[768,2048]{1,0:T(8,128)(2,1)} %bitcast.59, bf16[1,2048,256]{2,1,0:T(8,128)(2,1)S(1)} %copy-done), kind=kOutput, calls=%fused_computation.7 | convolution fusion | flops 805306368 | bytes 4980736 | tf_op jit(solution)/shard_map/dot_general | solution.py:803
  69.0 0.0 copy-done.1
  69.0 0.1 copy-done.4
  69.1 0.0 copy-start.3
  69.1 0.0 copy-start.5
  69.1 1.0 fusion.5
  70.1 0.9 copy-done.3
  71.0 0.3 copy-done.5
  71.2 1.2 multiply_convert_fusion.1
  72.4 2.4 %convolution_bitcast_fusion.2 = f32[1,2048,256]{2,1,0:T(8,128)} fusion(bf16[768,2048]{1,0:T(8,128)(2,1)S(1)} %bitcast.61, bf16[768,256]{1,0:T(8,128)(2,1)S(1)} %get-tuple-element.35), kind=kOutput, calls=%fused_computation.3 | convolution fusion | flops 805306368 | bytes 5636096 | tf_op jit(solution)/shard_map/rd,rf->df/dot_general | solution.py:814
  74.8 2.4 %convolution_bitcast_fusion.1 = f32[1,2048,256]{2,1,0:T(8,128)} fusion(bf16[768,2048]{1,0:T(8,128)(2,1)S(1)} %bitcast.62, bf16[768,256]{1,0:T(8,128)(2,1)S(1)} %get-tuple-element.34), kind=kOutput, calls=%fused_computation.2 | convolution fusion | flops 805306368 | bytes 5636096 | tf_op jit(solution)/shard_map/rd,rf->df/dot_general | solution.py:815
  77.2 2.4 %convolution_bitcast_fusion = f32[1,256,2048]{2,1,0:T(8,128)} fusion(bf16[768,2048]{1,0:T(8,128)(2,1)S(1)} %bitcast.58, f32[768,256]{1,0:T(8,128)S(1)} %fusion.5, f32[768,256]{1,0:T(8,128)S(1)} %fusion.2), kind=kOutput, calls=%fused_computation.1 | convolution fusion | flops 806486016 | bytes 6815744 | tf_op jit(solution)/shard_map/rf,rd->fd/dot_general | solution.py:813
  79.6 1.0 fusion
  80.6 0.0 copy-start.2
  80.6 2.7 %add_convert_fusion = bf16[768,2048]{1,0:T(8,128)(2,1)} fusion(f32[768,2048]{1,0:T(8,128)S(1)} %fusion, bf16[768,256]{1,0:T(8,128)(2,1)S(1)} %get-tuple-element.34, bf16[1,2048,256]{2,1,0:T(8,128)(2,1)S(1)} %copy-done.1), kind=kOutput, calls=%fused_computation | convolution fusion | flops 808452096 | bytes 10878976 | tf_op jit(solution)/shard_map/rf,df->rd/dot_general | solution.py:817
  83.3 0.0 copy-done.2
  83.3 0.1 fusion.10
  83.5 1.0 or_convert_fusion.pick
  84.5 43.8 %shard_map.191 = (bf16[192,2048]{1,0:T(8,128)(2,1)}, bf16[8,192,256]{2,1,0:T(8,128)(2,1)}) custom-call(bf16[8,96,2048]{2,1,0:T(8,128)(2,1)} %bitcast.47, bf16[8,192,96]{2,1,0:T(8,128)(2,1)} %or_convert_fusion.pick, bf16[192,256]{1,0:T(8,128)(2,1)} %get-tuple-element.22.branch), custom_call_target="tpu_custom_call" | custom-call | bytes 40000000 | tf_op jit(solution)/shard_map/pallas_call | solution.py:714
  128.2 0.0 copy-start.6
  128.3 24.2 %shard_map.192 = (bf16[8,192,256]{2,1,0:T(8,128)(2,1)}, f32[192,256]{1,0:T(8,128)}, f32[192,256]{1,0:T(8,128)}) custom-call(bf16[192,2048]{1,0:T(8,128)(2,1)} %get-tuple-element.23.normed, bf16[192,2048]{1,0:T(8,128)(2,1)} %res.3, bf16[192,2048]{1,0:T(8,128)(2,1)} %cot.3, f32[1,2048]{1,0:T(1,128)} %bitcast.53, bf16[2048,256]{1,0:T(8,128)(2,1)} %proj.1, ...), custom_call_target="tpu_custom_call" | custom-call | bytes 20000000 | tf_op jit(solution)/shard_map/pallas_call | solution.py:494
  152.5 0.0 copy-done.6
  152.5 2.2 %convolution_bitcast_fusion.3 = f32[256,256]{1,0:T(8,128)} fusion(bf16[8,192,256]{2,1,0:T(8,128)(2,1)} %get-tuple-element.30, bf16[8,192,256]{2,1,0:T(8,128)(2,1)S(1)} %copy-done.6), kind=kOutput, calls=%fused_computation.4 | convolution fusion | flops 201326592 | bytes 1835008 | tf_op jit(solution)/shard_map/dot_general | solution.py:844
  154.7 1.6 %copy.41 = f32[192,256]{1,0:T(8,128)} copy(f32[192,256]{1,0:T(8,128)} %get-tuple-element.50) | data formatting | bytes 393216
  156.3 1.6 %copy.42 = f32[192,256]{1,0:T(8,128)} copy(f32[192,256]{1,0:T(8,128)} %get-tuple-element.51) | data formatting | bytes 393216
  (8 shorter events, 0.1 us)
Async XLA Ops:
  0.6 65.3 %copy-start = (bf16[1,2048,256]{2,1,0:T(8,128)(2,1)S(1)}, bf16[1,2048,256]{2,1,0:T(8,128)(2,1)}, u32[]{:S(2)}) copy-start(bf16[1,2048,256]{2,1,0:T(8,128)(2,1)} %param.20) | copy-start | bytes 3145732
  65.9 3.1 %copy-start.1 = (bf16[1,2048,256]{2,1,0:T(8,128)(2,1)S(1)}, bf16[1,2048,256]{2,1,0:T(8,128)(2,1)}, u32[]{:S(2)}) copy-start(bf16[1,2048,256]{2,1,0:T(8,128)(2,1)} %param.21) | copy-start | bytes 3145732
  65.9 3.2 %copy-start.4 = (bf16[8,96,2048]{2,1,0:T(8,128)(2,1)S(1)}, bf16[8,96,2048]{2,1,0:T(8,128)(2,1)}, u32[]{:S(2)}) copy-start(bf16[8,96,2048]{2,1,0:T(8,128)(2,1)} %get-tuple-element.20) | copy-start | bytes 9437188
  69.1 1.9 %copy-start.3 = (bf16[8,96,2048]{2,1,0:T(8,128)(2,1)S(1)}, bf16[8,96,2048]{2,1,0:T(8,128)(2,1)}, u32[]{:S(2)}) copy-start(bf16[8,96,2048]{2,1,0:T(8,128)(2,1)} %get-tuple-element.21) | copy-start | bytes 9437188
  69.1 2.2 %copy-start.5 = (bf16[1,256,2048]{2,1,0:T(8,128)(2,1)S(1)}, bf16[1,256,2048]{2,1,0:T(8,128)(2,1)}, u32[]{:S(2)}) copy-start(bf16[1,256,2048]{2,1,0:T(8,128)(2,1)} %param.22) | copy-start | bytes 3145732
  80.6 2.7 %copy-start.2 = (s32[192,2]{0,1:T(2,128)S(1)}, s32[192,2]{0,1:T(2,128)}, u32[]{:S(2)}) copy-start(s32[192,2]{0,1:T(2,128)} %param.18) | copy-start | bytes 4612
  128.2 24.2 %copy-start.6 = (bf16[8,192,256]{2,1,0:T(8,128)(2,1)S(1)}, bf16[8,192,256]{2,1,0:T(8,128)(2,1)}, u32[]{:S(2)}) copy-start(bf16[8,192,256]{2,1,0:T(8,128)(2,1)} %get-tuple-element.31) | copy-start | bytes 2359300

commit v3 on v2

--- a/solution.py
+++ b/solution.py
@@ -151,7 +151,30 @@
 
         lax.fori_loop(1, sp_count, one_first, 0)
 
-    return start, start_own, pass_own, relay, finish
+    def complete(i):
+        for a in range(count):
+            passed(2, a, i, beside, beside).wait_recv()
+            passed(3, a, i, facing, beside).wait_recv()
+
+    def finish_sends():
+        def one(i, carry):
+            for a in range(count):
+                passed(1, a, i, t, across).wait_send()
+                passed(2, a, i, t, beside).wait_send()
+                passed(3, a, i, across, beside).wait_send()
+            return carry
+
+        lax.fori_loop(0, sp_count, one, 0)
+
+        def one_first(i, carry):
+            for a in range(count):
+                first(a, i).wait_send()
+            return carry
+
+        lax.fori_loop(1, sp_count, one_first, 0)
+
+    steps = (landed, pass_on, pass_back, complete, finish_sends)
+    return start, start_own, pass_own, relay, finish, steps
 
 
 def spread_sems(sp_count, count):
@@ -183,9 +206,16 @@
     prev,
     soft,
     maps,
+    gate_w,
+    up_w,
+    down_w,
     rows_out,
     cot_out,
-    branch_out,
+    full,
+    branch_all,
+    hidden_out,
+    d_gate_out,
+    d_up_out,
     rate_factor,
     input_factor,
     direct_factor,
@@ -198,17 +228,36 @@
     scaled_first,
     scaled_second,
     pre_values,
+    rows_held,
+    cot_held,
+    branch_out,
+    part,
+    from_beside,
+    to_across,
+    from_across,
+    mine,
+    leaving,
+    arrived,
+    quarter,
     local_sem,
     send_sem,
     recv_sem,
+    back_send,
+    back_recv,
+    branch_send,
+    branch_recv,
+    last_send,
+    last_recv,
+    keep_sem,
+    own_sem,
 ):
     s, t, beside, across = my_place(tp_count)
     hail(sp_count, s, t, beside, across)
-    start, start_own, pass_own, relay, finish = spreading(
+    start, start_own, pass_own, relay, finish, steps = spreading(
         sp_count,
         tp_count,
         (send_rows, send_cot),
-        (rows_out, cot_out),
+        (rows_held, cot_held),
         True,
         local_sem,
         send_sem,
@@ -316,8 +365,228 @@
         return carry
 
     lax.fori_loop(0, tok_rows // step, forward, 0)
-    relay()
-    finish()
+    landed, pass_on, pass_back, complete, finish_sends = steps
+    facing = lax.rem(beside + tp_count // 2, tp_count)
+    half = sp_count // 2
+    s_twin = s + 1 - 2 * lax.rem(s, 2)
+    over_cols = (((1,), (1,)), ((), ()))
+
+    def cols_of(q):
+        return pl.ds(pl.multiple_of(q * width, width), width)
+
+    def source_of(i):
+        return lax.rem(s + sp_count - i, sp_count)
+
+    def branch_copy(j):
+        return remote(
+            branch_out,
+            branch_all.at[s],
+            branch_send.at[0, j],
+            branch_recv.at[0, j],
+            (lax.rem(s + 2 * j, sp_count), t),
+        )
+
+    def branch_twin(j):
+        block = branch_all.at[lax.rem(s + sp_count - 2 * j, sp_count)]
+        return remote(block, block, branch_send.at[1, j], branch_recv.at[1, j], (s_twin, t))
+
+    own_branch = pltpu.make_async_copy(branch_out, branch_all.at[s], own_sem.at[0])
+    own_branch.start()
+
+    def start_branch(j, carry):
+        branch_copy(j).start()
+        return carry
+
+    lax.fori_loop(1, half, start_branch, 0)
+
+    def kept(i):
+        source = source_of(i)
+        return (
+            pltpu.make_async_copy(rows_held.at[source], rows_out.at[source], keep_sem.at[0, i]),
+            pltpu.make_async_copy(cot_held.at[source], cot_out.at[source], keep_sem.at[1, i]),
+        )
+
+    def to_beside(i, k):
+        q = beside if k == 0 else facing
+        return remote(
+            part.at[source_of(i), :, cols_of(q)],
+            from_beside.at[k, source_of(i)],
+            back_send.at[k, i],
+            back_recv.at[k, i],
+            (s, beside),
+        )
+
+    def crossing(i):
+        return remote(
+            to_across.at[source_of(i)],
+            from_across.at[source_of(i)],
+            back_send.at[2, i],
+            back_recv.at[2, i],
+            (s, across),
+        )
+
+    def homeward(i):
+        return remote(
+            leaving.at[source_of(i)],
+            arrived.at[s],
+            back_send.at[3, i],
+            back_recv.at[3, i],
+            (source_of(i), t),
+        )
+
+    def expert(i):
+        complete(i)
+        for copy in kept(i):
+            copy.start()
+        source = source_of(i)
+        rows_in = rows_held[source]
+        gate_pre = jnp.dot(rows_in, gate_w[...], preferred_element_type=jnp.float32)
+        up_pre = jnp.dot(rows_in, up_w[...], preferred_element_type=jnp.float32)
+        d_hidden = lax.dot_general(
+            cot_held[source], down_w[...], over_cols, preferred_element_type=jnp.float32
+        )
+        gate_sig = jax.nn.sigmoid(gate_pre)
+        gate_act = gate_pre * gate_sig
+        d_up = (d_hidden * gate_act).astype(jnp.bfloat16)
+        d_gate = (d_hidden * up_pre * gate_sig * (1.0 + gate_pre * (1.0 - gate_sig))).astype(
+            jnp.bfloat16
+        )
+        hidden_out[source] = (gate_act * up_pre).astype(jnp.bfloat16)
+        d_up_out[source] = d_up
+        d_gate_out[source] = d_gate
+        back = lax.dot_general(d_gate, gate_w[...], over_cols, preferred_element_type=jnp.float32)
+        back = back + lax.dot_general(
+            d_up, up_w[...], over_cols, preferred_element_type=jnp.float32
+        )
+        part[source] = back.astype(jnp.bfloat16)
+        to_beside(i, 1).start()
+        to_beside(i, 0).start()
+
+    def cross(i):
+        to_beside(i, 1).wait_recv()
+        at = source_of(i)
+        total = part[at, :, cols_of(across)].astype(jnp.float32) + from_beside[1, at].astype(
+            jnp.float32
+        )
+        to_across[at] = total.astype(jnp.bfloat16)
+        crossing(i).start()
+        to_beside(i, 0).wait_recv()
+        mine[at] = part[at, :, cols_of(t)].astype(jnp.float32) + from_beside[0, at].astype(
+            jnp.float32
+        )
+
+    def leave(i):
+        crossing(i).wait_recv()
+        at = source_of(i)
+        total = (mine[at] + from_across[at].astype(jnp.float32)).astype(jnp.bfloat16)
+
+        @pl.when(i > 0)
+        def _():
+            leaving[at] = total
+            homeward(i).start()
+
+        @pl.when(i == 0)
+        def _():
+            arrived[s] = total
+
+    def turn(i, carry):
+        @pl.when((i >= 1) & (i < sp_count))
+        def _():
+            landed(i)
+            pass_on(i)
+
+        @pl.when((i >= 1) & (i < sp_count + 1))
+        def _():
+            pass_back(i - 1)
+
+        @pl.when((i >= 2) & (i < sp_count + 2))
+        def _():
+            expert(i - 2)
+
+        @pl.when((i >= 3) & (i < sp_count + 3))
+        def _():
+            cross(i - 3)
+
+        @pl.when(i >= 4)
+        def _():
+            leave(i - 4)
+
+        return carry
+
+    lax.fori_loop(0, sp_count + 4, turn, 0)
+    own_branch.wait()
+    branch_twin(0).start()
+
+    def pass_branch(j, carry):
+        branch_copy(j).wait_recv()
+        branch_twin(j).start()
+        return carry
+
+    lax.fori_loop(1, half, pass_branch, 0)
+
+    def gather_rows(source):
+        base = (source * cap).astype(jnp.float32)
+        chosen = jnp.where(slot_first - base == lanes, 1.0, 0.0)
+        chosen = chosen + jnp.where(slot_second - base == lanes, 1.0, 0.0)
+        return jnp.dot(
+            chosen.astype(jnp.bfloat16), arrived[source], preferred_element_type=jnp.float32
+        )
+
+    def add_in(i, total):
+        source = lax.rem(s + i, sp_count)
+        remote(
+            leaving.at[source],
+            arrived.at[source],
+            back_send.at[3, i],
+            back_recv.at[3, i],
+            (source, t),
+        ).wait_recv()
+        return total + gather_rows(source)
+
+    quarter[...] = lax.fori_loop(1, sp_count, add_in, gather_rows(s)).astype(jnp.bfloat16)
+
+    def gathered(kind, source, q, to):
+        return remote(
+            source, full.at[:, cols_of(q)], last_send.at[kind], last_recv.at[kind], (s, to)
+        )
+
+    own_quarter = pltpu.make_async_copy(quarter, full.at[:, cols_of(t)], own_sem.at[1])
+    gathered(0, quarter, t, across).start()
+    gathered(1, quarter, t, beside).start()
+    own_quarter.start()
+    gathered(0, quarter, across, across).wait_recv()
+    gathered(2, full.at[:, cols_of(across)], across, beside).start()
+    finish_sends()
+
+    def end(i, carry):
+        to_beside(i, 0).wait_send()
+        to_beside(i, 1).wait_send()
+        crossing(i).wait_send()
+        for copy in kept(i):
+            copy.wait()
+        return carry
+
+    lax.fori_loop(0, sp_count, end, 0)
+
+    def end_home(i, carry):
+        homeward(i).wait_send()
+        return carry
+
+    lax.fori_loop(1, sp_count, end_home, 0)
+
+    def end_branch(j, carry):
+        branch_copy(j).wait_send()
+        branch_twin(j).wait()
+        return carry
+
+    lax.fori_loop(1, half, end_branch, 0)
+    branch_twin(0).wait()
+    own_quarter.wait()
+    gathered(1, quarter, beside, beside).wait_recv()
+    gathered(2, full.at[:, cols_of(facing)], facing, beside).wait_recv()
+    gathered(0, quarter, t, across).wait_send()
+    gathered(1, quarter, t, beside).wait_send()
+    gathered(2, full.at[:, cols_of(across)], across, beside).wait_send()
 
 
 def dispatch(sp_count, tp_count, cap, operands, number):
@@ -325,14 +594,23 @@
     tok_rows, model_width = res.shape
     width = model_width // tp_count
     wide = jax.ShapeDtypeStruct((sp_count, cap, model_width), jnp.bfloat16)
+    units = jax.ShapeDtypeStruct((sp_count, cap, operands[-1].shape[0]), jnp.bfloat16)
     factor = jax.ShapeDtypeStruct(conv.shape, jnp.float32)
+    blocks = (sp_count, cap, width)
     vmem = pl.BlockSpec(memory_space=pltpu.VMEM)
     anywhere = pl.BlockSpec(memory_space=pl.ANY)
     return pl.pallas_call(
         functools.partial(dispatch_kernel, sp_count, tp_count),
-        out_shape=[wide, wide, jax.ShapeDtypeStruct(conv.shape, jnp.bfloat16)] + [factor] * 6,
+        out_shape=[
+            wide,
+            wide,
+            jax.ShapeDtypeStruct(res.shape, jnp.bfloat16),
+            jax.ShapeDtypeStruct((sp_count,) + conv.shape, jnp.bfloat16),
+        ]
+        + [units] * 3
+        + [factor] * 6,
         in_specs=[vmem] * len(operands),
-        out_specs=[anywhere] * 2 + [vmem] * 7,
+        out_specs=[anywhere] * 4 + [vmem] * 9,
         scratch_shapes=[
             pltpu.VMEM((sp_count, cap, width), jnp.bfloat16),
             pltpu.VMEM((sp_count, cap, width), jnp.bfloat16),
@@ -340,8 +618,29 @@
             pltpu.VMEM((tok_rows, width), jnp.bfloat16),
             pltpu.VMEM((tok_rows, width), jnp.bfloat16),
             pltpu.VMEM((tok_rows, 2 * conv.shape[1]), jnp.float32),
+            pltpu.VMEM((sp_count, cap, model_width), jnp.bfloat16),
+            pltpu.VMEM((sp_count, cap, model_width), jnp.bfloat16),
+            pltpu.VMEM(conv.shape, jnp.bfloat16),
+            pltpu.VMEM((sp_count, cap, model_width), jnp.bfloat16),
+            pltpu.VMEM((2,) + blocks, jnp.bfloat16),
+            pltpu.VMEM(blocks, jnp.bfloat16),
+            pltpu.VMEM(blocks, jnp.bfloat16),
+            pltpu.VMEM(blocks, jnp.float32),
+            pltpu.VMEM(blocks, jnp.bfloat16),
+            pltpu.VMEM(blocks, jnp.bfloat16),
+            pltpu.VMEM((tok_rows, width), jnp.bfloat16),
         ]
-        + spread_sems(sp_count, 2),
+        + spread_sems(sp_count, 2)
+        + [
+            pltpu.SemaphoreType.DMA((4, sp_count)),
+            pltpu.SemaphoreType.DMA((4, sp_count)),
+            pltpu.SemaphoreType.DMA((2, sp_count // 2)),
+            pltpu.SemaphoreType.DMA((2, sp_count // 2)),
+            pltpu.SemaphoreType.DMA((3,)),
+            pltpu.SemaphoreType.DMA((3,)),
+            pltpu.SemaphoreType.DMA((2, sp_count)),
+            pltpu.SemaphoreType.DMA((2,)),
+        ],
         compiler_params=pltpu.CompilerParams(collective_id=number, has_side_effects=True),
         cost_estimate=pl.CostEstimate(flops=0, bytes_accessed=40_000_000, transcendentals=0),
     )(*operands)
@@ -377,7 +676,7 @@
 ):
     s, t, beside, across = my_place(tp_count)
     hail(sp_count, s, t, beside, across)
-    start, start_own, pass_own, relay, finish = spreading(
+    start, start_own, pass_own, relay, finish, steps = spreading(
         sp_count, tp_count, (share,), (mix_out,), False, local_sem, send_sem, recv_sem
     )
     tok_rows, model_width = res.shape
@@ -513,237 +812,6 @@
     )(*operands)
 
 
-def return_kernel(
-    sp_count,
-    tp_count,
-    part,
-    pick,
-    branch,
-    full,
-    branch_all,
-    from_beside,
-    to_across,
-    from_across,
-    mine,
-    leaving,
-    arrived,
-    quarter,
-    send_sem,
-    recv_sem,
-    branch_send,
-    branch_recv,
-    last_send,
-    last_recv,
-    local_sem,
-):
-    s, t, beside, across = my_place(tp_count)
-    facing = lax.rem(beside + tp_count // 2, tp_count)
-    width = quarter.shape[1]
-    half = sp_count // 2
-    s_twin = s + 1 - 2 * lax.rem(s, 2)
-
-    def cols(q):
-        return pl.ds(pl.multiple_of(q * width, width), width)
-
-    def place(i):
-        return lax.rem(s + i + 1, sp_count)
-
-    def to_beside(i, k):
-        q = beside if k == 0 else facing
-        return remote(
-            part.at[place(i), :, cols(q)],
-            from_beside.at[k, place(i)],
-            send_sem.at[k, i],
-            recv_sem.at[k, i],
-            (s, beside),
-        )
-
-    def crossing(i):
-        return remote(
-            to_across.at[place(i)],
-            from_across.at[place(i)],
-            send_sem.at[2, i],
-            recv_sem.at[2, i],
-            (s, across),
-        )
-
-    def homeward(i):
-        return remote(
-            leaving.at[place(i)],
-            arrived.at[s],
-            send_sem.at[3, i],
-            recv_sem.at[3, i],
-            (place(i), t),
-        )
-
-    def branch_out_copy(j):
-        return remote(
-            branch,
-            branch_all.at[s],
-            branch_send.at[0, j],
-            branch_recv.at[0, j],
-            (lax.rem(s + 2 * j, sp_count), t),
-        )
-
-    def branch_twin(j):
-        block = branch_all.at[lax.rem(s + sp_count - 2 * j, sp_count)]
-        return remote(block, block, branch_send.at[1, j], branch_recv.at[1, j], (s_twin, t))
-
-    greet(sp_count, s, t, beside, across)
-
-    def start_beside(i, carry):
-        to_beside(i, 1).start()
-        to_beside(i, 0).start()
-        return carry
-
-    lax.fori_loop(0, sp_count, start_beside, 0)
-    own_branch = pltpu.make_async_copy(branch, branch_all.at[s], local_sem.at[0])
-    own_branch.start()
-
-    def start_branch(j, carry):
-        branch_out_copy(j).start()
-        return carry
-
-    lax.fori_loop(1, half, start_branch, 0)
-
-    def cross(i):
-        to_beside(i, 1).wait_recv()
-        at = place(i)
-        total = part[at, :, cols(across)].astype(jnp.float32) + from_beside[1, at].astype(
-            jnp.float32
-        )
-        to_across[at] = total.astype(jnp.bfloat16)
-        crossing(i).start()
-        to_beside(i, 0).wait_recv()
-        mine[at] = part[at, :, cols(t)].astype(jnp.float32) + from_beside[0, at].astype(
-            jnp.float32
-        )
-
-    def total_of(i):
-        crossing(i).wait_recv()
-        at = place(i)
-        return (mine[at] + from_across[at].astype(jnp.float32)).astype(jnp.bfloat16)
-
-    def leave(i):
-        leaving[place(i)] = total_of(i)
-        homeward(i).start()
-
-    cross(0)
-    cross(1)
-
-    def middle(i, carry):
-        cross(i)
-        leave(i - 2)
-        return carry
-
-    lax.fori_loop(2, sp_count, middle, 0)
-    own_branch.wait()
-    branch_twin(0).start()
-    leave(sp_count - 2)
-    arrived[s] = total_of(sp_count - 1)
-
-    def pass_branch(j, carry):
-        branch_out_copy(j).wait_recv()
-        branch_twin(j).start()
-        return carry
-
-    lax.fori_loop(1, half, pass_branch, 0)
-
-    quarter_sum = jnp.dot(pick[s], arrived[s], preferred_element_type=jnp.float32)
-
-    def add_in(i, total):
-        source = lax.rem(s + 2 * sp_count - i - 1, sp_count)
-        remote(
-            leaving.at[source],
-            arrived.at[source],
-            send_sem.at[3, i],
-            recv_sem.at[3, i],
-            (source, t),
-        ).wait_recv()
-        return total + jnp.dot(pick[source], arrived[source], preferred_element_type=jnp.float32)
-
-    quarter_sum = lax.fori_loop(0, sp_count - 1, add_in, quarter_sum)
-    quarter[...] = quarter_sum.astype(jnp.bfloat16)
-
-    def gathered(kind, source, q, to):
-        return remote(
-            source, full.at[:, cols(q)], last_send.at[kind], last_recv.at[kind], (s, to)
-        )
-
-    own_quarter = pltpu.make_async_copy(quarter, full.at[:, cols(t)], local_sem.at[1])
-    gathered(0, quarter, t, across).start()
-    gathered(1, quarter, t, beside).start()
-    own_quarter.start()
-    gathered(0, quarter, across, across).wait_recv()
-    gathered(2, full.at[:, cols(across)], across, beside).start()
-
-    def finish(i, carry):
-        to_beside(i, 0).wait_send()
-        to_beside(i, 1).wait_send()
-        crossing(i).wait_send()
-        return carry
-
-    lax.fori_loop(0, sp_count, finish, 0)
-
-    def finish_home(i, carry):
-        homeward(i).wait_send()
-        return carry
-
-    lax.fori_loop(0, sp_count - 1, finish_home, 0)
-
-    def finish_branch(j, carry):
-        branch_out_copy(j).wait_send()
-        branch_twin(j).wait()
-        return carry
-
-    lax.fori_loop(1, half, finish_branch, 0)
-    branch_twin(0).wait()
-    own_quarter.wait()
-    gathered(1, quarter, beside, beside).wait_recv()
-    gathered(2, full.at[:, cols(facing)], facing, beside).wait_recv()
-    gathered(0, quarter, t, across).wait_send()
-    gathered(1, quarter, t, beside).wait_send()
-    gathered(2, full.at[:, cols(across)], across, beside).wait_send()
-
-
-def give_back(sp_count, tp_count, part, pick, branch, number):
-    cap, model_width = part.shape[1:]
-    width = model_width // tp_count
-    rows = branch.shape[0]
-    blocks = (sp_count, cap, width)
-    return pl.pallas_call(
-        functools.partial(return_kernel, sp_count, tp_count),
-        out_shape=[
-            jax.ShapeDtypeStruct((rows, model_width), jnp.bfloat16),
-            jax.ShapeDtypeStruct((sp_count,) + branch.shape, branch.dtype),
-        ],
-        in_specs=[
-            pl.BlockSpec(memory_space=pltpu.VMEM),
-            pl.BlockSpec(memory_space=pltpu.VMEM),
-            pl.BlockSpec(memory_space=pl.ANY),
-        ],
-        out_specs=[pl.BlockSpec(memory_space=pl.ANY)] * 2,
-        scratch_shapes=[
-            pltpu.VMEM((2,) + blocks, jnp.bfloat16),
-            pltpu.VMEM(blocks, jnp.bfloat16),
-            pltpu.VMEM(blocks, jnp.bfloat16),
-            pltpu.VMEM(blocks, jnp.float32),
-            pltpu.VMEM(blocks, jnp.bfloat16),
-            pltpu.VMEM(blocks, jnp.bfloat16),
-            pltpu.VMEM((rows, width), jnp.bfloat16),
-            pltpu.SemaphoreType.DMA((4, sp_count)),
-            pltpu.SemaphoreType.DMA((4, sp_count)),
-            pltpu.SemaphoreType.DMA((2, sp_count // 2)),
-            pltpu.SemaphoreType.DMA((2, sp_count // 2)),
-            pltpu.SemaphoreType.DMA((3,)),
-            pltpu.SemaphoreType.DMA((3,)),
-            pltpu.SemaphoreType.DMA((2,)),
-        ],
-        compiler_params=pltpu.CompilerParams(collective_id=number, has_side_effects=True),
-        cost_estimate=pl.CostEstimate(flops=0, bytes_accessed=40_000_000, transcendentals=0),
-    )(part, pick, branch)
-
-
 def per_device(
     cotangent,
     residual,
@@ -779,7 +847,7 @@
     maps = jnp.concatenate([whole_map(rate_map), whole_map(input_map)], axis=1)
     gain_row = norm_gain[None, :]
     soft_decay = jax.nn.softplus(-decay_param)[None, :]
-    rows_in, cot_in, branch_out, *factors = dispatch(
+    rows_in, cot_in, d_normed, branch_all, hidden, d_gate, d_up, *factors = dispatch(
         sp_count,
         tp_count,
         block_rows,
@@ -794,47 +862,20 @@
             prev_state,
             soft_decay,
             maps,
+            expert_gate[0],
+            expert_up[0],
+            expert_down[0],
         ),
         1,
     )
     rows_in = rows_in.reshape(slot_total, model_width)
     cot_in = cot_in.reshape(slot_total, model_width)
-    gate_w, up_w, down_w = expert_gate[0], expert_up[0], expert_down[0]
-    gate_pre = jnp.dot(rows_in, gate_w, preferred_element_type=jnp.float32)
-    up_pre = jnp.dot(rows_in, up_w, preferred_element_type=jnp.float32)
-    gate_sig = jax.nn.sigmoid(gate_pre)
-    gate_act = gate_pre * gate_sig
-    hidden = (gate_act * up_pre).astype(jnp.bfloat16)
-    d_hidden = jnp.einsum("rd,fd->rf", cot_in, down_w, preferred_element_type=jnp.float32)
-    d_up = (d_hidden * gate_act).astype(jnp.bfloat16)
-    d_gate = (d_hidden * up_pre * gate_sig * (1.0 + gate_pre * (1.0 - gate_sig))).astype(
-        jnp.bfloat16
-    )
+    hidden = hidden.reshape(slot_total, hidden.shape[2])
+    d_gate = d_gate.reshape(hidden.shape)
+    d_up = d_up.reshape(hidden.shape)
     grad_down = jnp.einsum("rf,rd->fd", hidden, cot_in, preferred_element_type=jnp.float32)[None]
     grad_gate = jnp.einsum("rd,rf->df", rows_in, d_gate, preferred_element_type=jnp.float32)[None]
     grad_up = jnp.einsum("rd,rf->df", rows_in, d_up, preferred_element_type=jnp.float32)[None]
-    back_terms = jnp.einsum("rf,df->rd", d_gate, gate_w, preferred_element_type=jnp.float32)
-    back_terms = back_terms + jnp.einsum("rf,df->rd", d_up, up_w, preferred_element_type=jnp.float32)
-    back_terms = back_terms.astype(jnp.bfloat16).reshape(sp_count, block_rows, model_width)
-    expert_hits = (
-        route_ids[:, :, None] == jnp.arange(experts_all, dtype=jnp.int32)[None, None, :]
-    ).astype(jnp.float32)
-    token = jnp.arange(tok_rows, dtype=jnp.int32)
-    earlier = (token[:, None] > token[None, :]).astype(jnp.bfloat16)
-    ranks = jnp.dot(
-        earlier,
-        jnp.sum(expert_hits, axis=1).astype(jnp.bfloat16),
-        preferred_element_type=jnp.float32,
-    )
-    slot_pair = route_ids * capacity + jnp.sum(ranks[:, None, :] * expert_hits, axis=2).astype(
-        jnp.int32
-    )
-    slots = jnp.arange(slot_total, dtype=jnp.int32)
-    slot_grid = slots.reshape(sp_count, 1, block_rows)
-    pick = (
-        (slot_grid == slot_pair[None, :, 0:1]) | (slot_grid == slot_pair[None, :, 1:2])
-    ).astype(jnp.bfloat16)
-    d_normed, branch_all = give_back(sp_count, tp_count, back_terms, pick, branch_out, 2)
     mix_cols, grad_conv_out, grad_branch_gate = tail(
         sp_count,
         tp_count,

time: 158 us -> 140 us (0.89)
  matrix products: 18.4 us -> 9.48 us
  Pallas kernels: 126 us -> 121 us
  local copies, waits for them, and re-layouts: 9.56 us -> 6.33 us
    pallas_call x1 -> x0, Pallas kernels: 43.8 us -> none  [give_back(): pl.pallas_call(functools.partial(return_kernel, sp_count, tp_count), out_...]
    pallas_call x1, Pallas kernels: 58.1 us -> 99.7 us  [dispatch(): pl.pallas_call(functools.partial(dispatch_kernel, sp_count, tp_count), ou...]
    dot_general x6 -> x0, matrix products: 9.07 us -> none  [the longest x1 3.02 us: per_device(): gate_pre = jnp.dot(rows_in, gate_w, preferred_element_type=jnp.float32)]
    unnamed x18, local copies, waits for them, and re-layouts: 7.5 us -> 4.27 us
    pallas_call x1, Pallas kernels: 24.2 us -> 21.7 us  [tail(): pl.pallas_call(functools.partial(tail_kernel, sp_count, tp_count), out_sh...]
where the time goes in v3:
time: 140 us
  Pallas kernels  121 us (86%)
  matrix products  9.48 us (7%)
  local copies, waits for them, and re-layouts  6.33 us (5%)
  other arithmetic  2.09 us (1%)
    pallas_call x1, Pallas kernels, dispatch(): pl.pallas_call(functools.partial(dispatch_kernel, sp_count, tp_count), ou...  99.7 us
    pallas_call x1, Pallas kernels, tail(): pl.pallas_call(functools.partial(tail_kernel, sp_count, tp_count), out_sh...  21.7 us
    unnamed x18, local copies, waits for them, and re-layouts  4.27 us

profile of v3, /device:TPU:0, one launch (start us, length us, event | category | flops | bytes accessed | tf_op | source)
XLA Modules:
  0.0 140.1 jit_solution(1346174105242022555)
XLA Ops:
  0.6 1.3 compare_select_fusion.2
  1.9 0.9 copy.23
  2.8 0.9 copy.25
  3.8 0.1 copy.26
  3.9 0.1 copy.24
  4.0 0.1 compare_select_fusion.1
  4.1 0.7 pad_maximum_fusion.maps
  4.8 1.4 %copy.27.ids = s32[192,2]{1,0:T(8,128)} copy(s32[192,2]{0,1:T(2,128)} %param.18) | data formatting | bytes 3072 | tf_op args[3]
  6.3 1.4 %copy.28.weights = f32[192,2]{1,0:T(8,128)} copy(f32[192,2]{0,1:T(2,128)} %param.19) | data formatting | bytes 3072 | tf_op args[4]
  7.7 99.7 %shard_map.190 = (bf16[8,96,2048]{2,1,0:T(8,128)(2,1)}, bf16[8,96,2048]{2,1,0:T(8,128)(2,1)}, bf16[192,2048]{1,0:T(8,128)(2,1)}, bf16[8,192,256]{2,1,0:T(8,128)(...) custom-call(bf16[192,2048]{1,0:T(8,128)(2,1)} %res.3, ...), custom_call_target="tpu_custom_call" | custom-call | bytes 40000000 | tf_op jit(solution)/shard_map/pallas_call | solution.py:602
  107.5 0.0 copy-start.3
  107.5 0.0 copy-start.6
  107.5 21.7 %shard_map.191 = (bf16[8,192,256]{2,1,0:T(8,128)(2,1)}, f32[192,256]{1,0:T(8,128)}, f32[192,256]{1,0:T(8,128)}) custom-call(bf16[192,2048]{1,0:T(8,128)(2,1)} %get-tuple-element.27.normed, bf16[192,2048]{1,0:T(8,128)(2,1)} %res.3, bf16[192,2048]{1,0:T(8,128)(2,1)} %cot.3, f32[1,2048]{1,0:T(1,128)} %bitcast.36, bf16[2048,256]{1,0:T(8,128)(2,1)} %proj.1, ...), custom_call_target="tpu_custom_call" | custom-call | bytes 20000000 | tf_op jit(solution)/shard_map/pallas_call | solution.py:793
  129.2 2.5 %convolution_bitcast_fusion.3 = f32[256,256]{1,0:T(8,128)} fusion(bf16[8,192,256]{2,1,0:T(8,128)(2,1)} %get-tuple-element.34, bf16[8,192,256]{2,1,0:T(8,128)(2,1)} %get-tuple-element.35), kind=kOutput, calls=%fused_computation.3 | convolution fusion | flops 201326592 | bytes 1835008 | tf_op jit(solution)/shard_map/dot_general | solution.py:885
  131.7 0.0 copy-done.3
  131.7 0.0 copy-done.6
  131.7 0.0 copy-start.5
  131.7 2.3 %convolution_bitcast_fusion.2 = f32[1,2048,256]{2,1,0:T(8,128)} fusion(bf16[8,96,2048]{2,1,0:T(8,128)(2,1)S(1)} %copy-done.3, bf16[8,96,256]{2,1,0:T(8,128)(2,1)S(1)} %copy-done.6), kind=kOutput, calls=%fused_computation.2 | convolution fusion | flops 805306368 | bytes 5636096 | tf_op jit(solution)/shard_map/rd,rf->df/dot_general | solution.py:877
  134.1 0.0 copy-done.5
  134.1 0.0 copy-start.2
  134.1 0.0 copy-start.4
  134.1 2.3 %convolution_bitcast_fusion.1 = f32[1,2048,256]{2,1,0:T(8,128)} fusion(bf16[8,96,2048]{2,1,0:T(8,128)(2,1)S(1)} %copy-done.3, bf16[8,96,256]{2,1,0:T(8,128)(2,1)S(1)} %copy-done.5), kind=kOutput, calls=%fused_computation.1 | convolution fusion | flops 805306368 | bytes 5636096 | tf_op jit(solution)/shard_map/rd,rf->df/dot_general | solution.py:878
  136.4 0.0 copy-done.2
  136.4 0.0 copy-done.4
  136.4 0.0 copy-start.1
  136.4 0.0 copy-start
  136.4 2.3 %convolution_bitcast_fusion = f32[1,256,2048]{2,1,0:T(8,128)} fusion(bf16[8,96,256]{2,1,0:T(8,128)(2,1)S(1)} %copy-done.4, bf16[8,96,2048]{2,1,0:T(8,128)(2,1)S(1)} %copy-done.2), kind=kOutput, calls=%fused_computation | convolution fusion | flops 805306368 | bytes 5636096 | tf_op jit(solution)/shard_map/rf,rd->fd/dot_general | solution.py:876
  138.7 0.0 copy-done.1
  138.7 0.7 copy.31
  139.4 0.0 copy-done
  139.4 0.7 copy.32
  (3 shorter events, 0.0 us)
Async XLA Ops:
  107.5 24.3 %copy-start.3 = (bf16[8,96,2048]{2,1,0:T(8,128)(2,1)S(1)}, bf16[8,96,2048]{2,1,0:T(8,128)(2,1)}, u32[]{:S(2)}) copy-start(bf16[8,96,2048]{2,1,0:T(8,128)(2,1)} %get-tuple-element.22) | copy-start | bytes 9437188
  107.5 24.2 %copy-start.6 = (bf16[8,96,256]{2,1,0:T(8,128)(2,1)S(1)}, bf16[8,96,256]{2,1,0:T(8,128)(2,1)}, u32[]{:S(2)}) copy-start(bf16[8,96,256]{2,1,0:T(8,128)(2,1)} %get-tuple-element.23) | copy-start | bytes 1179652
  131.7 2.3 %copy-start.5 = (bf16[8,96,256]{2,1,0:T(8,128)(2,1)S(1)}, bf16[8,96,256]{2,1,0:T(8,128)(2,1)}, u32[]{:S(2)}) copy-start(bf16[8,96,256]{2,1,0:T(8,128)(2,1)} %get-tuple-element.24) | copy-start | bytes 1179652
  134.1 2.3 %copy-start.2 = (bf16[8,96,2048]{2,1,0:T(8,128)(2,1)S(1)}, bf16[8,96,2048]{2,1,0:T(8,128)(2,1)}, u32[]{:S(2)}) copy-start(bf16[8,96,2048]{2,1,0:T(8,128)(2,1)} %get-tuple-element.26) | copy-start | bytes 9437188
  134.1 2.3 %copy-start.4 = (bf16[8,96,256]{2,1,0:T(8,128)(2,1)S(1)}, bf16[8,96,256]{2,1,0:T(8,128)(2,1)}, u32[]{:S(2)}) copy-start(bf16[8,96,256]{2,1,0:T(8,128)(2,1)} %get-tuple-element.25) | copy-start | bytes 1179652
  136.4 2.3 %copy-start.1 = (f32[192,256]{1,0:T(8,128)S(1)}, f32[192,256]{1,0:T(8,128)}, u32[]{:S(2)}) copy-start(f32[192,256]{1,0:T(8,128)} %get-tuple-element.50) | copy-start | bytes 589828
  136.4 3.0 %copy-start = (f32[192,256]{1,0:T(8,128)S(1)}, f32[192,256]{1,0:T(8,128)}, u32[]{:S(2)}) copy-start(f32[192,256]{1,0:T(8,128)} %get-tuple-element.51) | copy-start | bytes 589828
